TPU v7x, 32 devices: a whole 2x2x4 slice. The times are simulated.
32 devices in a mesh: fs: 8 (over z, x), tp: 4 (over y, core).
Axes of the slice: x: 2, y: 2, z: 4, core: 2. Of those that a mesh axis runs over, the one named last changes fastest.
Arguments:
- tokens: bfloat16 [1024, 2048], P('fs'), may hold values from -6 to 6
- gain: float32 [2048], P('fs'), may hold values from 0.1 to 1.9
- up_master: float32 [2048, 8192], P('fs', 'tp'), may hold values from -0.125 to 0.125
- down_master: float32 [2048, 8192], P('fs', 'tp'), may hold values from -0.0625 to 0.0625
Outputs:
- up_sampled: bfloat16 [8, 2048, 1024], P('fs', None, 'tp')
- down_sampled: bfloat16 [8, 2048, 1024], P('fs', None, 'tp')
- mixed: bfloat16 [1024, 2048], P('fs', 'tp')
All inputs are finite; a program needn't handle non-finite values.
Results may differ from a plain program's by a relative error of at most 0.0087.
Values may be sent and summed in bfloat16 or wider, within the bound.
A program may use at most 64 MiB of HBM per device.

v0:
```python
import functools

import jax
import jax.numpy as jnp
from jax import lax
from jax.experimental import pallas as pl
from jax.experimental.pallas import tpu as pltpu
from jax.sharding import PartitionSpec as P

SUB = 8
EPS = 1e-06
BF16 = jnp.bfloat16
F32 = jnp.float32


def fused(
    nz, tok_h, gain, upm_h, dnm_h, up_h, dn_h, mix_o,
    tok, upm, dnm, up_o, dn_o, s_in, s_out, xg, up_s, dn_s, act, cs, cr, fw, fb, yr, gs, gb, gr, hb, hr, xs, xb, xr, kept, zb, zr,
    s_tz, r_tz, s_tx, r_tx, s_ty, r_ty, s_tc, r_tc,
    s_up, r_up, s_dn, r_dn, s_c, r_c, s_y, r_y, s_g, r_g, s_h, r_h, s_x, r_x, s_z, r_z,
):
    f, t = lax.axis_index("fs"), lax.axis_index("tp")
    z, x = f // 2, f % 2
    y, c = t // 2, t % 2
    ox, oy, oc = 1 - x, 1 - y, 1 - c
    rows, width = tok.shape
    cols = width // 4
    feat = upm.shape[0]
    units = act.shape[1]
    at_x = (z * 2 + ox, t)
    at_y = (f, oy * 2 + c)
    at_c = (f, y * 2 + oc)

    fetch = [pltpu.make_async_copy(src, dst, s_in.at[n]) for n, (src, dst) in enumerate(
        ((tok_h, tok), (upm_h, upm), (dnm_h, dnm)))]
    for copy in fetch:
        copy.start()

    barrier = pltpu.get_barrier_semaphore()
    for d in range(1, SUB):
        pl.semaphore_signal(barrier, inc=1, device_id=((f + d) % SUB, t),
                            device_id_type=pl.DeviceIdType.MESH)
    for dev in (at_y, at_c):
        pl.semaphore_signal(barrier, inc=1, device_id=dev, device_id_type=pl.DeviceIdType.MESH)

    sent = []

    def send(src, dst, ssem, rsem, dev):
        copy = pltpu.make_async_remote_copy(
            src_ref=src, dst_ref=dst, send_sem=ssem, recv_sem=rsem,
            device_id=dev, device_id_type=pl.DeviceIdType.MESH)
        copy.start()
        sent.append(copy)

    def arrived(dst, ssem, rsem, dev):
        pltpu.make_async_remote_copy(
            src_ref=dst, dst_ref=dst, send_sem=ssem, recv_sem=rsem,
            device_id=dev, device_id_type=pl.DeviceIdType.MESH).wait_recv()

    low = 1 - z // 2
    far = (3 * low, 1 + low, 1 - z + 4 * (1 - low))

    turn = (far[0] * c + far[2] * (1 - c), far[1], far[2] * c + far[0] * (1 - c))

    fetch[0].wait()
    wide = tok[...].astype(F32)
    scale = lax.rsqrt(jnp.mean(wide * wide, axis=1, keepdims=True) + EPS)
    mine = tok[:, pl.ds(pl.multiple_of(t * cols, cols), cols)].astype(F32)
    xg[t, z, x] = (mine * scale).astype(BF16)
    pl.semaphore_wait(barrier, SUB + 1)

    for zz in turn:
        send(xg.at[t, z, x], xg.at[t, z, x], s_tz.at[zz], r_tz.at[z], (zz * 2 + x, t))

    def pass_on(zz):
        send(xg.at[t, zz, x], xg.at[t, zz, x], s_tx.at[zz], r_tx.at[zz], at_x)
        send(xg.at[t, zz, x], xg.at[t, zz, x], s_ty.at[zz, x], r_ty.at[zz, x], at_y)

    pass_on(z)

    def cast(src, dst, out, factor):
        for m in range(SUB):
            block = src[:, m * units:(m + 1) * units]
            dst[m] = (block if factor is None else factor * block).astype(BF16)
        block = src[:, pl.ds(pl.multiple_of(f * units, units), units)]
        out[pl.ds(pl.multiple_of(f * feat, feat), feat), :] = (
            block if factor is None else factor * block).astype(BF16)

    def at_rows(ref, k):
        return ref.at[pl.ds(pl.multiple_of(k * feat, feat), feat), :]

    def order(planes):
        return [z * 2 + ox] + [zz * 2 + xx for zz in planes for xx in (x, ox)]

    fine = feat // 2

    def at_half(ref, k, i):
        return ref.at[pl.ds(pl.multiple_of(k * feat + i * fine, fine), fine), :]

    fetch[1].wait()
    cast(upm, up_s, up_o, jnp.transpose(gain[...]))
    for dest in order(turn):
        send(up_s.at[dest], at_rows(up_o, f), s_up.at[dest], r_up.at[f], (dest, t))
    fetch[2].wait()
    cast(dnm, dn_s, dn_o, None)

    near = (far[2], far[1], far[0])
    for zz in near:
        arrived(xg.at[t, zz, x], s_tz.at[zz], r_tz.at[zz], (zz * 2 + x, t))
        pass_on(zz)
    for xx in (x,):
        send(xg.at[t, :, xx], xg.at[t, :, xx], s_tc.at[y, xx], r_tc.at[y, xx], at_c)
    for zz in (z,) + near:
        arrived(xg.at[t, zz, ox], s_tx.at[zz], r_tx.at[zz], at_x)
        send(xg.at[t, zz, ox], xg.at[t, zz, ox], s_ty.at[zz, ox], r_ty.at[zz, ox], at_y)
    send(xg.at[t, :, ox], xg.at[t, :, ox], s_tc.at[y, ox], r_tc.at[y, ox], at_c)
    other = oy * 2 + c
    for xx in (x, ox):
        for zz in (z,) + near:
            arrived(xg.at[other, zz, xx], s_ty.at[zz, xx], r_ty.at[zz, xx], at_y)
        send(xg.at[other, :, xx], xg.at[other, :, xx], s_tc.at[oy, xx], r_tc.at[oy, xx], at_c)
    def send_down(i, dest):
        send(dn_s.at[dest, i * fine:(i + 1) * fine], at_half(dn_o, f, i),
             s_dn.at[i, dest], r_dn.at[i, f], (dest, t))

    for i in range(2):
        for dest in order(far[2:]):
            send_down(i, dest)
    for yy in (y, oy):
        for xx in (x, ox):
            part = xg.at[yy * 2 + oc, :, xx]
            arrived(part, s_tc.at[yy, xx], r_tc.at[yy, xx], at_c)

    everyone = [zz * 2 + xx for zz in far for xx in (x, ox)] + [z * 2 + ox]
    for k in everyone:
        arrived(at_rows(up_o, k), s_up.at[k], r_up.at[k], (k, t))
    crossing = (far[0] * c + far[1] * (1 - c), far[1] * c + far[0] * (1 - c))
    for i in range(2):
        for zz in crossing:
            for xx in (x, ox):
                send_down(i, zz * 2 + xx)
    keep_up = pltpu.make_async_copy(up_o, up_h, s_out.at[0])
    keep_up.start()

    span = 2 * rows

    @pl.loop(0, nz)
    def _(zz):
        total = jnp.zeros((span, units), F32)
        for q in range(4):
            total += jnp.dot(xg[q, zz].reshape(span, cols), up_o[q * cols:(q + 1) * cols, :],
                             preferred_element_type=F32)
        act[pl.ds(pl.multiple_of(zz * span, span), span), :] = jnp.square(
            jnp.maximum(total, 0.0)).astype(BF16)

    def partial(yy, cc, i, zz):
        rows_act = act[pl.ds(pl.multiple_of(zz * span, span), span), :]
        return jnp.concatenate([
            lax.dot_general(
                rows_act, at_half(dn_o, yy * 4 + cc * 2 + xx, i)[...],
                (((1,), (1,)), ((), ())), preferred_element_type=F32)
            for xx in range(2)], axis=1)

    def have(yy, cc, i):
        for xx in range(2):
            k = yy * 4 + cc * 2 + xx

            @pl.when(k != f)
            def _():
                arrived(at_half(dn_o, k, i), s_dn.at[i, k], r_dn.at[i, k], (k, t))

    def two(h):
        return pl.ds(h * 2, 2)

    def each(h, body):
        @pl.loop(0, 2)
        def _(step):
            body(h * 2 + step)

    def to_core(yy, i):
        have(yy, oc, i)

        @pl.loop(0, nz)
        def _(zz):
            cs[yy * 2 + i, zz] = partial(yy, oc, i, zz).astype(BF16)

        send(cs.at[yy * 2 + i], cr.at[yy * 2 + i], s_c.at[yy, i], r_c.at[yy, i], at_c)

    def core_sum(yy, i, zz):
        return partial(yy, c, i, zz) + cr[yy * 2 + i, zz].astype(F32)

    def halves(total, wide_ref, sent_ref, zz):
        for xx in range(2):
            half = total[xx * rows:(xx + 1) * rows]
            wide_ref[xx, zz] = half
            sent_ref[xx, zz] = half.astype(BF16)

    hs = (low, 1 - low)
    close = z // 2
    over_y = [
        pltpu.make_async_remote_copy(
            src_ref=fb.at[oy, two(h)], dst_ref=yr.at[two(h)], send_sem=s_y.at[h],
            recv_sem=r_y.at[h], device_id=at_y, device_id_type=pl.DeviceIdType.MESH)
        for h in hs]
    sent.extend(over_y)

    def stage(i, yy):
        to_core(yy, i)
        have(yy, c, i)
        arrived(cr.at[yy * 2 + i], s_c.at[yy, i], r_c.at[yy, i], at_c)
        for h in hs:
            if i == 1:
                each(h, lambda zz: halves(core_sum(yy, 1, zz), gs.at[yy], gb.at[yy], zz))
                send(gb.at[yy, ox, two(h)], gr.at[yy, two(h)],
                     s_g.at[yy, h], r_g.at[yy, h], at_x)
            else:
                def body(zz):
                    total = core_sum(yy, 0, zz)
                    fw[yy, zz] = total
                    fb[yy, zz] = total.astype(BF16)

                each(h, body)
        if i == 0:
            @pl.when(yy == oy)
            def _():
                for copy in over_y:
                    copy.start()

    pair, same = far[2], (z + 2) % 4
    across = (pair + 2) % 4
    at_pair, at_same = (pair * 2 + x, t), (same * 2 + x, t)

    def to_pair(i, place):
        if place == 0:
            send(zb.at[i, across], zr.at[i, 0], s_z.at[i, 0], r_z.at[i, 0], at_pair)
        else:
            send(zb.at[i, pair], zr.at[i, 1], s_z.at[i, 1], r_z.at[i, 1], at_pair)

    def cross(i):
        arrived(zr.at[i, 0], s_z.at[i, 0], r_z.at[i, 0], at_pair)
        zb[i, z] = (kept[i, same] + zr[i, 0].astype(F32)).astype(BF16)
        send(zb.at[i, z], zr.at[i, 2], s_z.at[i, 2], r_z.at[i, 2], at_same)

    over_h = [
        pltpu.make_async_remote_copy(
            src_ref=hb.at[two(h)], dst_ref=hr.at[two(h)], send_sem=s_h.at[h],
            recv_sem=r_h.at[h], device_id=at_y, device_id_type=pl.DeviceIdType.MESH)
        for h in hs]
    sent.extend(over_h)

    def other_half():
        for place, h in enumerate(hs):
            arrived(gr.at[oy, two(h)], s_g.at[oy, h], r_g.at[oy, h], at_x)

            def body(zz):
                hb[zz] = (gs[oy, x, zz] + gr[oy, zz].astype(F32)).astype(BF16)

            each(h, body)
            over_h[place].start()

    stage(0, close)
    stage(1, close)
    stage(0, 1 - close)
    pl.when(oy == close)(other_half)
    stage(1, 1 - close)
    for h in hs:
        arrived(yr.at[two(h)], s_y.at[h], r_y.at[h], at_y)
        each(h, lambda zz: halves(fw[y, zz] + yr[zz].astype(F32), xs, xb, zz))
        send(xb.at[ox, two(h)], xr.at[two(h)], s_x.at[h], r_x.at[h], at_x)
    pl.when(oy != close)(other_half)
    keep_dn = pltpu.make_async_copy(dn_o, dn_h, s_out.at[1])
    keep_dn.start()
    for place, h in enumerate(hs):
        arrived(xr.at[two(h)], s_x.at[h], r_x.at[h], at_x)

        def body(zz):
            total = xs[x, zz] + xr[zz].astype(F32)
            kept[0, zz] = total

            @pl.when(zz != z)
            def _():
                zb[0, zz] = total.astype(BF16)

        each(h, body)
        to_pair(0, place)
    cross(0)
    for place, h in enumerate(hs):
        arrived(gr.at[y, two(h)], s_g.at[y, h], r_g.at[y, h], at_x)
        arrived(hr.at[two(h)], s_h.at[h], r_h.at[h], at_y)

        def body(zz):
            total = gs[y, x, zz] + gr[y, zz].astype(F32) + hr[zz].astype(F32)
            kept[1, zz] = total

            @pl.when(zz != z)
            def _():
                zb[1, zz] = total.astype(BF16)

        each(h, body)
        to_pair(1, place)
        if place == 0:
            cross(1)
    for i in range(2):
        arrived(zr.at[i, 1], s_z.at[i, 1], r_z.at[i, 1], at_pair)
        arrived(zr.at[i, 2], s_z.at[i, 2], r_z.at[i, 2], at_same)
        total = (kept[i, z] + zr[i, 1].astype(F32) + zr[i, 2].astype(F32)).astype(BF16)
        for xx in range(2):
            mix_o[:, xx * feat + i * fine:xx * feat + (i + 1) * fine] = (
                total[:, xx * fine:(xx + 1) * fine])
    for copy in sent:
        copy.wait_send()
    keep_up.wait()
    keep_dn.wait()


def on_device_fused(tokens, gain, up_master, down_master):
    rows, width = tokens.shape
    feat, ff = up_master.shape
    units = ff // SUB
    nz = SUB // 2
    cols = width // 4
    span = 2 * rows
    dma = pltpu.SemaphoreType.DMA
    vmem = pl.BlockSpec(memory_space=pltpu.VMEM)
    anywhere = pl.BlockSpec(memory_space=pl.ANY)
    shapes = [(nz,), (nz,), (nz, 2), (2, 2), (SUB,), (2, SUB), (2, 2), (2,), (2, 2), (2,), (2,), (2, nz)]
    up_s, dn_s, mixed = pl.pallas_call(
        functools.partial(fused, nz),
        out_shape=(
            jax.ShapeDtypeStruct((SUB * feat, units), BF16),
            jax.ShapeDtypeStruct((SUB * feat, units), BF16),
            jax.ShapeDtypeStruct((rows, cols), BF16),
        ),
        in_specs=[anywhere, vmem, anywhere, anywhere],
        out_specs=(anywhere, anywhere, vmem),
        scratch_shapes=[
            pltpu.VMEM((rows, width), BF16),
            pltpu.VMEM((feat, ff), F32),
            pltpu.VMEM((feat, ff), F32),
            pltpu.VMEM((SUB * feat, units), BF16),
            pltpu.VMEM((SUB * feat, units), BF16),
            dma((3,)),
            dma((2,)),
            pltpu.VMEM((4, nz, 2, rows, cols), BF16),
            pltpu.VMEM((SUB, feat, units), BF16),
            pltpu.VMEM((SUB, feat, units), BF16),
            pltpu.VMEM((SUB * rows, units), BF16),
            pltpu.VMEM((4, nz, span, feat), BF16),
            pltpu.VMEM((4, nz, span, feat), BF16),
            pltpu.VMEM((2, nz, span, feat), F32),
            pltpu.VMEM((2, nz, span, feat), BF16),
            pltpu.VMEM((nz, span, feat), BF16),
            pltpu.VMEM((2, 2, nz, rows, feat), F32),
            pltpu.VMEM((2, 2, nz, rows, feat), BF16),
            pltpu.VMEM((2, nz, rows, feat), BF16),
            pltpu.VMEM((nz, rows, feat), BF16),
            pltpu.VMEM((nz, rows, feat), BF16),
            pltpu.VMEM((2, nz, rows, feat), F32),
            pltpu.VMEM((2, nz, rows, feat), BF16),
            pltpu.VMEM((nz, rows, feat), BF16),
            pltpu.VMEM((2, nz, rows, feat), F32),
            pltpu.VMEM((2, nz, rows, feat), BF16),
            pltpu.VMEM((2, nz, rows, feat), BF16),
        ] + [dma(shape) for shape in shapes for _ in range(2)],
        compiler_params=pltpu.CompilerParams(
            collective_id=0, has_side_effects=True, vmem_limit_bytes=60 * 2**20),
    )(tokens, gain[None, :], up_master, down_master)
    return up_s[None], dn_s[None], mixed


def from_partner(block, axis, bit):
    count = lax.axis_size(axis)
    route = []
    for low in range(count):
        high = low | 1 << bit
        if high != low and high < count:
            route += [(low, high), (high, low)]
    return lax.ppermute(block, axis, route)


def on_device(tokens, gain, up_master, down_master):
    fs_count = lax.axis_size("fs")
    feat_rows = up_master.shape[0]
    units = up_master.shape[1] // SUB
    groups_count = fs_count // SUB
    member = lax.axis_index("fs") % SUB
    up_round = (gain[:, None] * up_master).astype(jnp.bfloat16)
    down_round = down_master.astype(jnp.bfloat16)

    def spread(weight):
        blocks = weight.reshape(feat_rows, SUB, units).transpose(1, 0, 2)
        return jnp.broadcast_to(blocks[None], (groups_count, SUB, feat_rows, units)).reshape(
            fs_count, feat_rows, units
        )

    up_sampled, down_sampled = (
        lax.all_to_all(spread(up_round), "fs", split_axis=0, concat_axis=1, tiled=True),
        lax.all_to_all(spread(down_round), "fs", split_axis=0, concat_axis=1, tiled=True),
    )
    levels = SUB.bit_length() - 1
    bit_list = list(range(levels))
    widened = tokens.astype(jnp.float32)
    normed = (
        widened * lax.rsqrt(jnp.mean(widened * widened, axis=1, keepdims=True) + 1e-06)
    ).astype(jnp.bfloat16)
    current = normed[None]
    for bit in bit_list:
        partner = from_partner(current, "fs", bit)
        lower = member >> bit & 1 == 0
        current = jnp.where(lower, jnp.stack([current, partner]), jnp.stack([partner, current]))
    order_now = list(reversed(bit_list))
    wanted = list(range(levels - 1, -1, -1))
    perm_axes = [
        [place for place, value in enumerate(order_now) if value == target][0] for target in wanted
    ]
    current = jnp.transpose(current, perm_axes + [levels, levels + 1, levels + 2])
    gathered = current.reshape(SUB * tokens.shape[0], tokens.shape[1])
    pre_units = jnp.dot(gathered, up_sampled[0], preferred_element_type=jnp.float32)
    act_units = jnp.square(jax.nn.relu(pre_units)).astype(jnp.bfloat16)
    partial_out = lax.dot_general(
        act_units, down_sampled[0], (((1,), (1,)), ((), ())), preferred_element_type=jnp.float32
    )
    running = partial_out.reshape((2,) * levels + (tokens.shape[0], tokens.shape[1]))
    axis_bits = list(range(levels - 1, -1, -1))
    for bit in bit_list:
        position = len([value for value in axis_bits if value > bit])
        mine = member >> bit & 1
        keep = lax.dynamic_index_in_dim(running, mine, position, keepdims=False)
        other = lax.dynamic_index_in_dim(running, 1 - mine, position, keepdims=False)
        running = keep + from_partner(other, "fs", bit)
        axis_bits = [value for value in axis_bits if value != bit]
    summed = lax.psum_scatter(running, "tp", scatter_dimension=1, tiled=True)
    return (up_sampled, down_sampled, summed.astype(jnp.bfloat16))


def solution(mesh):
    placed = (P("fs", None), P("fs"), P("fs", "tp"), P("fs", "tp"))
    one_group = mesh.shape["fs"] == SUB and mesh.shape["tp"] == 4
    return jax.shard_map(
        on_device_fused if one_group else on_device,
        mesh=mesh,
        in_specs=placed,
        out_specs=(P("fs", None, "tp"), P("fs", None, "tp"), P("fs", "tp")),
        check_vma=False,
    )
```

profile of v0, /device:TPU:0, one launch (start us, length us, event | category | flops | bytes accessed | tf_op | source)
XLA Modules:
  0.0 96.7 jit_solution(12488166744574095489)
XLA Ops:
  0.6 92.1 %shard_map.67 = (bf16[2048,256]{1,0:T(8,128)(2,1)}, bf16[2048,256]{1,0:T(8,128)(2,1)}, bf16[128,512]{1,0:T(8,128)(2,1)}) custom-call(bf16[128,2048]{1,0:T(8,128)(2,1)} %tok_h.1, f32[1,256]{1,0:T(1,128)} %bitcast.5, f32[256,2048]{1,0:T(8,128)} %upm_h.1, f32[256,2048]{1,0:T(8,128)} %dnm_h.1), custom_call_target="tpu_custom_call" | custom-call | tf_op jit(solution)/shard_map/pallas_call | solution.py:327
  92.7 0.0 copy-start
  92.7 0.0 copy-start.1
  92.7 2.4 %copy.10 = bf16[1,2048,256]{2,1,0:T(8,128)(2,1)} copy(bf16[1,2048,256]{2,1,0:T(8,128)(2,1)} %bitcast.4) | data formatting | bytes 2097152
  95.1 0.0 copy-done
  95.1 1.0 %copy.11 = bf16[1,2048,256]{2,1,0:T(8,128)(2,1)} copy(bf16[1,2048,256]{2,1,0:T(8,128)(2,1)S(1)} %bitcast.3) | data formatting | bytes 2097152
  96.1 0.0 copy-done.1
  96.1 0.7 copy.12
Async XLA Ops:
  92.7 2.4 %copy-start = (bf16[2048,256]{1,0:T(8,128)(2,1)S(1)}, bf16[2048,256]{1,0:T(8,128)(2,1)}, u32[]{:S(2)}) copy-start(bf16[2048,256]{1,0:T(8,128)(2,1)} %get-tuple-element.7) | copy-start | bytes 3145732
  92.7 3.3 %copy-start.1 = (bf16[128,512]{1,0:T(8,128)(2,1)S(1)}, bf16[128,512]{1,0:T(8,128)(2,1)}, u32[]{:S(2)}) copy-start(bf16[128,512]{1,0:T(8,128)(2,1)} %get-tuple-element.14) | copy-start | bytes 393220
where the time goes:
time: 96.9 us; the launch traced here: 96.7 us
  Pallas kernels  92.1 us (95%)
  local copies, waits for them, and re-layouts  3.99 us (4%)
    pallas_call x1, Pallas kernels, on_device_fused(): pl.pallas_call(functools.partial(fused, nz), out_shape=(jax.ShapeDtypeStr...  92.1 us
    unnamed x7, local copies, waits for them, and re-layouts  3.99 us

commit v1 on v0

v1 whole, which is shorter than its diff:
```python
import functools
import types

import jax
import jax.numpy as jnp
from jax import lax
from jax.experimental import pallas as pl
from jax.experimental.pallas import tpu as pltpu
from jax.sharding import PartitionSpec as P

SUB = 8
EPS = 1e-06
BF16 = jnp.bfloat16
F32 = jnp.float32
PIECES = 4


def fused(nz, names, tok_h, gain, upm_h, dnm_h, up_h, dn_h, mix_o, *refs):
    r = types.SimpleNamespace(**dict(zip(names, refs)))
    mark = jax.named_scope
    f, t = lax.axis_index("fs"), lax.axis_index("tp")
    z, x = f // 2, f % 2
    y, c = t // 2, t % 2
    ox, oy, oc = 1 - x, 1 - y, 1 - c
    rows, width = r.tok.shape
    cols = width // nz
    feat = r.upm.shape[0]
    units = r.act.shape[1]
    fine = feat // PIECES
    wide = 2 * fine
    span = 2 * rows
    close = z // 2
    same = (z + 2) % 4
    pair = z + 1 - 2 * (z % 2)
    across = (pair + 2) % 4
    inner = 2 - close
    central = jnp.logical_or(z == 1, z == 2)
    at_x = (z * 2 + ox, t)
    at_y = (f, oy * 2 + c)
    at_c = (f, y * 2 + oc)

    def at_z(zz):
        return (zz * 2 + x, t)

    fetch = [pltpu.make_async_copy(src, dst, r.s_in.at[n]) for n, (src, dst) in enumerate(
        ((tok_h, r.tok), (upm_h, r.upm), (dnm_h, r.dnm)))]
    for copy in fetch:
        copy.start()

    barrier = pltpu.get_barrier_semaphore()
    partners = (at_z(pair), at_z(same), at_z(across), at_x, at_y, at_c)
    for dev in partners:
        pl.semaphore_signal(barrier, inc=1, device_id=dev, device_id_type=pl.DeviceIdType.MESH)

    sent = []

    def remote(src, dst, ssem, rsem, dev):
        return pltpu.make_async_remote_copy(
            src_ref=src, dst_ref=dst, send_sem=ssem, recv_sem=rsem,
            device_id=dev, device_id_type=pl.DeviceIdType.MESH)

    def send(src, dst, ssem, rsem, dev):
        copy = remote(src, dst, ssem, rsem, dev)
        copy.start()
        sent.append((copy, None))

    def prepare(src, dst, ssem, rsem, dev, when):
        copy = remote(src, dst, ssem, rsem, dev)
        sent.append((copy, when))
        return copy

    def arrived(dst, ssem, rsem, dev):
        remote(dst, dst, ssem, rsem, dev).wait_recv()

    def at_rows(ref, k):
        return ref.at[pl.ds(pl.multiple_of(k * feat, feat), feat), :]

    def at_piece(ref, k, p):
        return ref.at[pl.ds(pl.multiple_of(k * feat + p * fine, fine), fine), :]

    def cast(src, dst, out, factor):
        for m in range(SUB):
            block = src[:, m * units:(m + 1) * units]
            dst[m] = (block if factor is None else factor * block).astype(BF16)
        block = src[:, pl.ds(pl.multiple_of(f * units, units), units)]
        out[pl.ds(pl.multiple_of(f * feat, feat), feat), :] = (
            block if factor is None else factor * block).astype(BF16)

    with mark("norm"):
        fetch[0].wait()
        full = r.tok[...].astype(F32)
        scale = lax.rsqrt(jnp.mean(full * full, axis=1, keepdims=True) + EPS)
        for q in range(nz):
            r.xg[q, z, x] = (full[:, q * cols:(q + 1) * cols] * scale).astype(BF16)
    with mark("castup"):
        fetch[1].wait()
        cast(r.upm, r.up_s, r.up_o, jnp.transpose(gain[...]))
    with mark("barrier"):
        pl.semaphore_wait(barrier, len(partners))

    def token_x(zz):
        part = r.xg.at[t, zz, x]
        send(part, part, r.s_tx.at[zz], r.r_tx.at[zz], at_x)

    def token_y(zz, xx):
        part = r.xg.at[t, zz, xx]
        send(part, part, r.s_ty.at[zz, xx], r.r_ty.at[zz, xx], at_y)

    def token_c(yy, zz, xx):
        part = r.xg.at[yy * 2 + c, zz, xx]
        send(part, part, r.s_tc.at[yy, zz, xx], r.r_tc.at[yy, zz, xx], at_c)

    def up_x(zz):
        send(r.up_s.at[zz * 2 + ox], r.up_r.at[zz], r.s_ux.at[zz], r.r_ux.at[zz], at_x)

    def up_own(zz):
        send(r.up_s.at[zz * 2 + x], at_rows(r.up_o, f), r.s_up.at[zz], r.r_up.at[f], at_z(zz))

    def up_relay(zz):
        arrived(r.up_r.at[zz], r.s_ux.at[zz], r.r_ux.at[zz], at_x)
        send(r.up_r.at[zz], at_rows(r.up_o, z * 2 + ox), r.s_ur.at[zz], r.r_up.at[z * 2 + ox], at_z(zz))

    def slab(p):
        return pl.ds(p * fine, fine)

    def dn_x(zz, p):
        send(r.dn_s.at[zz * 2 + ox, slab(p)], r.dn_r.at[zz, slab(p)],
             r.s_dx.at[zz, p], r.r_dx.at[zz, p], at_x)

    def dn_own(p):
        for zz in (same, across):
            send(r.dn_s.at[zz * 2 + x, slab(p)], at_piece(r.dn_o, f, p),
                 r.s_dl.at[0, zz, p], r.r_dl.at[f, p], at_z(zz))

    def dn_relay(p):
        for zz in (same, across):
            got = r.dn_r.at[zz, slab(p)]
            arrived(got, r.s_dx.at[zz, p], r.r_dx.at[zz, p], at_x)
            send(got, at_piece(r.dn_o, z * 2 + ox, p),
                 r.s_dl.at[1, zz, p], r.r_dl.at[z * 2 + ox, p], at_z(zz))

    own = r.xg.at[t, z, x]
    send(own, own, r.s_tz.at[0], r.r_tz.at[z], at_z(inner))
    send(own, own, r.s_tz.at[1], r.r_tz.at[z], at_z(pair))
    token_x(z)
    up_own(pair)
    for zz in (same, across):
        up_x(zz)
    for zz in (same, across):
        up_own(zz)
    with mark("castdn"):
        fetch[2].wait()
        cast(r.dnm, r.dn_s, r.dn_o, None)
    passed = [
        prepare(r.xg.at[t, zz, x], r.xg.at[t, zz, x], r.s_tz.at[2 + n], r.r_tz.at[zz], at_z(pair), central)
        for n, zz in enumerate((same, across))]

    def token_in(zz):
        token_x(zz)
        token_y(zz, x)
        token_c(y, zz, x)

    with mark("tokpair"):
        arrived(r.xg.at[t, pair, x], r.s_tz.at[0], r.r_tz.at[pair], at_z(pair))
        token_in(pair)
    with mark("toktx0"):
        arrived(r.xg.at[t, z, ox], r.s_tx.at[z], r.r_tx.at[z], at_x)
        token_y(z, ox)
        token_c(y, z, ox)
    up_x(pair)

    def far_tokens():
        for n, zz in enumerate((same, across)):
            arrived(r.xg.at[t, zz, x], r.s_tz.at[0], r.r_tz.at[zz], at_z(pair))

    with mark("tokfarc"):
        @pl.when(central)
        def _():
            far_tokens()
            for copy in passed:
                copy.start()

    with mark("uprelay"):
        for zz in (same, across):
            up_relay(zz)
    with mark("tokfare"):
        pl.when(jnp.logical_not(central))(far_tokens)
        for zz in (same, across):
            token_in(zz)
    send(r.up_s.at[z * 2 + ox], at_rows(r.up_o, f), r.s_up.at[z], r.r_up.at[f], at_x)
    send(r.dn_s.at[pair * 2 + ox], r.dn_r.at[pair], r.s_dx.at[pair, 0], r.r_dx.at[pair, 0], at_x)
    send(r.dn_s.at[z * 2 + ox], at_rows(r.dn_o, f), r.s_de.at[2], r.r_de.at[f], at_x)
    for p in range(PIECES):
        for zz in (same, across):
            dn_x(zz, p)
    with mark("uppair"):
        up_relay(pair)
    send(r.dn_s.at[pair * 2 + x], at_rows(r.dn_o, f), r.s_de.at[0], r.r_de.at[f], at_z(pair))
    for zz in (pair, same, across):
        with mark("toktx"):
            arrived(r.xg.at[t, zz, ox], r.s_tx.at[zz], r.r_tx.at[zz], at_x)
            token_y(zz, ox)
            token_c(y, zz, ox)
    dn_own(0)
    other = oy * 2 + c
    blocks = ((pair, x), (z, ox), (same, x), (across, x), (pair, ox), (same, ox), (across, ox))
    for zz, xx in blocks:
        with mark("tokty"):
            arrived(r.xg.at[other, zz, xx], r.s_ty.at[zz, xx], r.r_ty.at[zz, xx], at_y)
            token_c(oy, zz, xx)
    with mark("dnpair"):
        arrived(r.dn_r.at[pair], r.s_dx.at[pair, 0], r.r_dx.at[pair, 0], at_x)
        send(r.dn_r.at[pair], at_rows(r.dn_o, z * 2 + ox), r.s_de.at[1], r.r_de.at[z * 2 + ox], at_z(pair))
    with mark("dnrel0"):
        dn_relay(0)
    with mark("toktc"):
        for yy in (y, oy):
            for zz, xx in blocks:
                part = r.xg.at[yy * 2 + oc, zz, xx]
                arrived(part, r.s_tc.at[yy, zz, xx], r.r_tc.at[yy, zz, xx], at_c)

    def wait_up(zz, xx):
        k = zz * 2 + xx
        arrived(at_rows(r.up_o, k), r.s_up.at[z], r.r_up.at[k], at_x)

    def up_dot(q, zz):
        return jnp.dot(r.xg[q, zz].reshape(span, cols),
                       r.up_o[pl.ds(pl.multiple_of(q * cols, cols), cols), :],
                       preferred_element_type=F32)

    def at_span(zz):
        return pl.ds(pl.multiple_of(zz * span, span), span)

    with mark("upnear"):
        wait_up(z, ox)
        wait_up(pair, x)
        wait_up(pair, ox)
    with mark("mmnear"):
        @pl.loop(0, nz)
        def _(zz):
            r.pre[at_span(zz), :] = up_dot(close * 2, zz) + up_dot(close * 2 + 1, zz)
    with mark("dnfar1"):
        dn_own(1)
        dn_relay(1)
    with mark("upfar"):
        for zz in (same, across):
            for xx in (x, ox):
                wait_up(zz, xx)
    with mark("mmfar"):
        @pl.loop(0, nz)
        def _(zz):
            low = (1 - close) * 2
            total = r.pre[at_span(zz), :] + up_dot(low, zz) + up_dot(low + 1, zz)
            r.act[at_span(zz), :] = jnp.square(jnp.maximum(total, 0.0)).astype(BF16)
    keep_up = pltpu.make_async_copy(r.up_o, up_h, r.s_out.at[0])
    keep_up.start()

    mine = (y == close, y != close)
    not_mine = (mine[1], mine[0])
    at_pair, at_same = at_z(pair), at_z(same)

    def block_of(u):
        q, part = UNITS[u]
        if part == "far":
            return q, 2 * (1 - close), 2
        if part == "near":
            return q, 2 * close, 2
        return q, 0, nz

    def product(u):
        q, base, n = block_of(u)
        yy, p = (close if q < PIECES else 1 - close), q % PIECES
        if q == 0:
            for zz, xx in ((z, ox), (pair, x), (pair, ox)):
                k = zz * 2 + xx
                arrived(at_rows(r.dn_o, k), r.s_de.at[0], r.r_de.at[k], at_x)
        elif q >= PIECES and UNITS[u][1] != "near":
            for zz in (same, across):
                for xx in (x, ox):
                    k = zz * 2 + xx
                    arrived(at_piece(r.dn_o, k, p), r.s_dl.at[0, zz, p], r.r_dl.at[k, p], at_x)
        taken = jnp.concatenate(
            [at_piece(r.dn_o, yy * 4 + cc * 2 + xx, p)[...] for cc in (oc, c) for xx in range(2)], axis=0)
        total = lax.dot_general(
            r.act[pl.ds(pl.multiple_of(base * span, span), n * span), :], taken,
            (((1,), (1,)), ((), ())), preferred_element_type=F32)
        at = pl.ds(base, n)
        r.cs[q, at] = total[:, :wide].astype(BF16).reshape(n, 2, rows, wide)
        r.part[q, at] = total[:, wide:].reshape(n, 2, rows, wide)
        send(r.cs.at[q, at], r.cr.at[q, at], r.s_c.at[u], r.r_c.at[u], at_c)

    def over(base, n, body):
        @pl.loop(0, n)
        def _(i):
            body(base + i)

    def core_sum(u):
        q, base, n = block_of(u)
        at = pl.ds(base, n)
        arrived(r.cr.at[q, at], r.s_c.at[u], r.r_c.at[u], at_c)
        if q not in Y_FIRST:
            def body(zz):
                r.xb[q, zz] = (r.part[q, zz, ox] + r.cr[q, zz, ox].astype(F32)).astype(BF16)
                r.xs[q, zz] = r.part[q, zz, x] + r.cr[q, zz, x].astype(F32)

            over(base, n, body)
            send(r.xb.at[q, at], r.xr.at[q, at], r.s_x.at[u], r.r_x.at[u], at_x)
        else:
            theirs = not_mine[q // PIECES]
            over_y = prepare(r.fb.at[q, at], r.fr.at[q, at], r.s_y.at[u], r.r_y.at[u], at_y, theirs)

            @pl.when(theirs)
            def _():
                def body(zz):
                    r.fb[q, zz] = (r.part[q, zz] + r.cr[q, zz].astype(F32)).astype(BF16)

                over(base, n, body)
                over_y.start()

    def first_sum(u):
        q, base, n = block_of(u)
        at = pl.ds(base, n)
        if q not in Y_FIRST:
            theirs = not_mine[q // PIECES]
            arrived(r.xr.at[q, at], r.s_x.at[u], r.r_x.at[u], at_x)
            over_y = prepare(r.yb.at[q, at], r.yr.at[q, at], r.s_y.at[u], r.r_y.at[u], at_y, theirs)

            @pl.when(theirs)
            def _():
                def body(zz):
                    r.yb[q, zz] = (r.xs[q, zz] + r.xr[q, zz].astype(F32)).astype(BF16)

                over(base, n, body)
                over_y.start()
        else:
            ours = mine[q // PIECES]
            over_x = prepare(r.xb.at[q, at], r.xr.at[q, at], r.s_x.at[u], r.r_x.at[u], at_x, ours)

            @pl.when(ours)
            def _():
                arrived(r.fr.at[q, at], r.s_y.at[u], r.r_y.at[u], at_y)

                def body(zz):
                    def whole(xx):
                        return (r.part[q, zz, xx] + r.cr[q, zz, xx].astype(F32)
                                + r.fr[q, zz, xx].astype(F32))

                    r.xb[q, zz] = whole(ox).astype(BF16)
                    r.xs[q, zz] = whole(x)

                over(base, n, body)
                over_x.start()

    def second_sum(u):
        q, base, n = block_of(u)
        at, ours, p = pl.ds(base, n), mine[q // PIECES], q % PIECES
        part = UNITS[u][1]
        to_pair = [
            prepare(r.zb.at[p, who], r.zr.at[p, m], r.s_z.at[p, m], r.r_z.at[p, m], at_pair, ours)
            for m, who in ((0, across), (1, pair)) if part != ("near", "far")[m]]

        @pl.when(ours)
        def _():
            if q in Y_FIRST:
                arrived(r.xr.at[q, at], r.s_x.at[u], r.r_x.at[u], at_x)
            else:
                arrived(r.yr.at[q, at], r.s_y.at[u], r.r_y.at[u], at_y)

            def body(zz):
                total = r.xs[q, zz] + r.xr[q, zz].astype(F32)
                if q not in Y_FIRST:
                    total = total + r.yr[q, zz].astype(F32)
                r.kept[p, zz] = total
                r.zb[p, zz] = total.astype(BF16)

            over(base, n, body)
            for copy in to_pair:
                copy.start()

    def cross_sum(u):
        q = UNITS[u][0]
        ours, p = mine[q // PIECES], q % PIECES
        over_z = prepare(r.zc.at[p], r.zr.at[p, 2], r.s_z.at[p, 2], r.r_z.at[p, 2], at_same, ours)

        @pl.when(ours)
        def _():
            arrived(r.zr.at[p, 0], r.s_z.at[p, 0], r.r_z.at[p, 0], at_pair)
            r.zc[p] = (r.kept[p, same] + r.zr[p, 0].astype(F32)).astype(BF16)
            over_z.start()

    def more_down(p):
        dn_own(p)
        dn_relay(p)

    stages = dict(a=product, b=core_sum, c=first_sum, d=second_sum, e=cross_sum, D=more_down)
    for step in ORDER:
        with mark("st_" + step):
            stages[step[0]](int(step[1]))
    keep_dn = pltpu.make_async_copy(r.dn_o, dn_h, r.s_out.at[1])
    keep_dn.start()
    for p in range(PIECES):
        with mark("final%d" % p):
            arrived(r.zr.at[p, 1], r.s_z.at[p, 1], r.r_z.at[p, 1], at_pair)
            arrived(r.zr.at[p, 2], r.s_z.at[p, 2], r.r_z.at[p, 2], at_same)
            total = (r.kept[p, z] + r.zr[p, 1].astype(F32) + r.zr[p, 2].astype(F32)).astype(BF16)
            for xx in range(2):
                mix_o[:, xx * feat + p * fine:xx * feat + (p + 1) * fine] = total[:, xx * fine:(xx + 1) * fine]
    with mark("drain"):
        for copy, when in sent:
            if when is None:
                copy.wait_send()
            else:
                pl.when(when)(copy.wait_send)
        keep_up.wait()
        keep_dn.wait()


UNITS = tuple((q, "all") for q in range(7)) + ((7, "far"), (7, "near"))
Y_FIRST = (0, 4)
ORDER = (
    "a0", "a1", "b0", "a2", "b1", "a3", "b2", "b3", "D2", "a4", "b4", "D3", "c1", "c2", "c0", "a5", "b5",
    "c3", "d1", "c4", "d2", "d0", "a6", "b6", "c5", "d3", "d4", "a7", "a8", "b7", "b8", "c6", "e1", "e2", "e0", "e3",
    "d5", "e4", "c7", "c8", "d6", "e5", "d7", "e6", "d8", "e7",
)


def on_device_fused(tokens, gain, up_master, down_master):
    rows, width = tokens.shape
    feat, ff = up_master.shape
    units = ff // SUB
    nz = SUB // 2
    cols = width // nz
    fine = feat // PIECES
    wide = 2 * fine
    n, pieces = len(UNITS), 2 * PIECES
    dma = pltpu.SemaphoreType.DMA
    vmem = pl.BlockSpec(memory_space=pltpu.VMEM)
    anywhere = pl.BlockSpec(memory_space=pl.ANY)
    arrays = dict(
        tok=((rows, width), BF16), upm=((feat, ff), F32), dnm=((feat, ff), F32),
        up_o=((SUB * feat, units), BF16), dn_o=((SUB * feat, units), BF16),
        xg=((nz, nz, 2, rows, cols), BF16),
        up_s=((SUB, feat, units), BF16), dn_s=((SUB, feat, units), BF16),
        up_r=((nz, feat, units), BF16), dn_r=((nz, feat, units), BF16),
        pre=((SUB * rows, units), F32), act=((SUB * rows, units), BF16),
        cs=((pieces, nz, 2, rows, wide), BF16), cr=((pieces, nz, 2, rows, wide), BF16),
        part=((pieces, nz, 2, rows, wide), F32),
        xs=((pieces, nz, rows, wide), F32), xb=((pieces, nz, rows, wide), BF16), xr=((pieces, nz, rows, wide), BF16),
        yb=((pieces, nz, rows, wide), BF16), yr=((pieces, nz, rows, wide), BF16),
        fb=((pieces, nz, 2, rows, wide), BF16), fr=((pieces, nz, 2, rows, wide), BF16),
        kept=((PIECES, nz, rows, wide), F32), zb=((PIECES, nz, rows, wide), BF16),
        zc=((PIECES, rows, wide), BF16), zr=((PIECES, 3, rows, wide), BF16),
    )
    sems = dict(
        s_in=(3,), s_out=(2,), s_tz=(nz,), r_tz=(nz,), s_tx=(nz,), r_tx=(nz,), s_ty=(nz, 2), r_ty=(nz, 2),
        s_tc=(2, nz, 2), r_tc=(2, nz, 2), s_ux=(nz,), r_ux=(nz,), s_up=(nz,), r_up=(SUB,), s_ur=(nz,),
        s_dx=(nz, PIECES), r_dx=(nz, PIECES), s_de=(3,), r_de=(SUB,), s_dl=(2, nz, PIECES), r_dl=(SUB, PIECES),
        s_c=(n,), r_c=(n,), s_x=(n,), r_x=(n,), s_y=(n,), r_y=(n,), s_z=(PIECES, 3), r_z=(PIECES, 3),
    )
    names = list(arrays) + list(sems)
    up_s, dn_s, mixed = pl.pallas_call(
        functools.partial(fused, nz, names),
        out_shape=(
            jax.ShapeDtypeStruct((SUB * feat, units), BF16),
            jax.ShapeDtypeStruct((SUB * feat, units), BF16),
            jax.ShapeDtypeStruct((rows, cols), BF16),
        ),
        in_specs=[anywhere, vmem, anywhere, anywhere],
        out_specs=(anywhere, anywhere, vmem),
        scratch_shapes=[pltpu.VMEM(*spec) for spec in arrays.values()] + [dma(shape) for shape in sems.values()],
        compiler_params=pltpu.CompilerParams(
            collective_id=0, has_side_effects=True, vmem_limit_bytes=60 * 2**20),
    )(tokens, gain[None, :], up_master, down_master)
    return up_s[None], dn_s[None], mixed


def from_partner(block, axis, bit):
    count = lax.axis_size(axis)
    route = []
    for low in range(count):
        high = low | 1 << bit
        if high != low and high < count:
            route += [(low, high), (high, low)]
    return lax.ppermute(block, axis, route)


def on_device(tokens, gain, up_master, down_master):
    fs_count = lax.axis_size("fs")
    feat_rows = up_master.shape[0]
    units = up_master.shape[1] // SUB
    groups_count = fs_count // SUB
    member = lax.axis_index("fs") % SUB
    up_round = (gain[:, None] * up_master).astype(jnp.bfloat16)
    down_round = down_master.astype(jnp.bfloat16)

    def spread(weight):
        blocks = weight.reshape(feat_rows, SUB, units).transpose(1, 0, 2)
        return jnp.broadcast_to(blocks[None], (groups_count, SUB, feat_rows, units)).reshape(
            fs_count, feat_rows, units
        )

    up_sampled, down_sampled = (
        lax.all_to_all(spread(up_round), "fs", split_axis=0, concat_axis=1, tiled=True),
        lax.all_to_all(spread(down_round), "fs", split_axis=0, concat_axis=1, tiled=True),
    )
    levels = SUB.bit_length() - 1
    bit_list = list(range(levels))
    widened = tokens.astype(jnp.float32)
    normed = (
        widened * lax.rsqrt(jnp.mean(widened * widened, axis=1, keepdims=True) + 1e-06)
    ).astype(jnp.bfloat16)
    current = normed[None]
    for bit in bit_list:
        partner = from_partner(current, "fs", bit)
        lower = member >> bit & 1 == 0
        current = jnp.where(lower, jnp.stack([current, partner]), jnp.stack([partner, current]))
    order_now = list(reversed(bit_list))
    wanted = list(range(levels - 1, -1, -1))
    perm_axes = [
        [place for place, value in enumerate(order_now) if value == target][0] for target in wanted
    ]
    current = jnp.transpose(current, perm_axes + [levels, levels + 1, levels + 2])
    gathered = current.reshape(SUB * tokens.shape[0], tokens.shape[1])
    pre_units = jnp.dot(gathered, up_sampled[0], preferred_element_type=jnp.float32)
    act_units = jnp.square(jax.nn.relu(pre_units)).astype(jnp.bfloat16)
    partial_out = lax.dot_general(
        act_units, down_sampled[0], (((1,), (1,)), ((), ())), preferred_element_type=jnp.float32
    )
    running = partial_out.reshape((2,) * levels + (tokens.shape[0], tokens.shape[1]))
    axis_bits = list(range(levels - 1, -1, -1))
    for bit in bit_list:
        position = len([value for value in axis_bits if value > bit])
        mine = member >> bit & 1
        keep = lax.dynamic_index_in_dim(running, mine, position, keepdims=False)
        other = lax.dynamic_index_in_dim(running, 1 - mine, position, keepdims=False)
        running = keep + from_partner(other, "fs", bit)
        axis_bits = [value for value in axis_bits if value != bit]
    summed = lax.psum_scatter(running, "tp", scatter_dimension=1, tiled=True)
    return (up_sampled, down_sampled, summed.astype(jnp.bfloat16))


def solution(mesh):
    placed = (P("fs", None), P("fs"), P("fs", "tp"), P("fs", "tp"))
    one_group = mesh.shape["fs"] == SUB and mesh.shape["tp"] == 4
    return jax.shard_map(
        on_device_fused if one_group else on_device,
        mesh=mesh,
        in_specs=placed,
        out_specs=(P("fs", None, "tp"), P("fs", None, "tp"), P("fs", "tp")),
        check_vma=False,
    )
```

time: 96.9 us -> 88.1 us (0.909)
  Pallas kernels: 92.1 us -> 83.3 us
    pallas_call x1, Pallas kernels: 92.1 us -> 83.3 us  [on_device_fused(): pl.pallas_call(functools.partial(fused, nz, names), out_shape=(jax.ShapeD...]
where the time goes in v1:
time: 88.1 us; the launch traced here: 87.9 us
  Pallas kernels  83.3 us (95%)
  local copies, waits for them, and re-layouts  3.99 us (5%)
    pallas_call x1, Pallas kernels, on_device_fused(): pl.pallas_call(functools.partial(fused, nz, names), out_shape=(jax.ShapeD...  83.3 us
    unnamed x7, local copies, waits for them, and re-layouts  3.99 us

profile of v1, /device:TPU:0, one launch (start us, length us, event | category | flops | bytes accessed | tf_op | source)
XLA Modules:
  0.0 87.9 jit_solution(8220643337429219763)
XLA Ops:
  0.6 83.3 %shard_map.67 = (bf16[2048,256]{1,0:T(8,128)(2,1)}, bf16[2048,256]{1,0:T(8,128)(2,1)}, bf16[128,512]{1,0:T(8,128)(2,1)}) custom-call(bf16[128,2048]{1,0:T(8,128)(2,1)} %tok_h.1, f32[1,256]{1,0:T(1,128)} %bitcast.5, f32[256,2048]{1,0:T(8,128)} %upm_h.1, f32[256,2048]{1,0:T(8,128)} %dnm_h.1), custom_call_target="tpu_custom_call" | custom-call | tf_op jit(solution)/shard_map/pallas_call | solution.py:461
  83.9 0.0 copy-start
  83.9 0.0 copy-start.1
  83.9 2.4 %copy.10 = bf16[1,2048,256]{2,1,0:T(8,128)(2,1)} copy(bf16[1,2048,256]{2,1,0:T(8,128)(2,1)} %bitcast.4) | data formatting | bytes 2097152
  86.3 0.0 copy-done
  86.3 1.0 %copy.11 = bf16[1,2048,256]{2,1,0:T(8,128)(2,1)} copy(bf16[1,2048,256]{2,1,0:T(8,128)(2,1)S(1)} %bitcast.3) | data formatting | bytes 2097152
  87.2 0.0 copy-done.1
  87.2 0.7 copy.12
Async XLA Ops:
  83.9 2.4 %copy-start = (bf16[2048,256]{1,0:T(8,128)(2,1)S(1)}, bf16[2048,256]{1,0:T(8,128)(2,1)}, u32[]{:S(2)}) copy-start(bf16[2048,256]{1,0:T(8,128)(2,1)} %get-tuple-element.7) | copy-start | bytes 3145732
  83.9 3.3 %copy-start.1 = (bf16[128,512]{1,0:T(8,128)(2,1)S(1)}, bf16[128,512]{1,0:T(8,128)(2,1)}, u32[]{:S(2)}) copy-start(bf16[128,512]{1,0:T(8,128)(2,1)} %get-tuple-element.14) | copy-start | bytes 393220

commit v2 on v1

v2 whole, which is shorter than its diff:
```python
import collections
import functools
import math
import types

import jax
import jax.numpy as jnp
from jax import lax
from jax.experimental import pallas as pl
from jax.experimental.pallas import tpu as pltpu
from jax.sharding import PartitionSpec as P

SUB = 8
EPS = 1e-06
BF16 = jnp.bfloat16
F32 = jnp.float32
PIECES = 4


def fused(nz, names, tok_h, gain, upm_h, dnm_h, up_o, dn_o, mix_o, *refs):
    r = types.SimpleNamespace(**dict(zip(names, refs)))
    r.up_o, r.dn_o = up_o, dn_o
    mark = jax.named_scope
    f, t = lax.axis_index("fs"), lax.axis_index("tp")
    z, x = f // 2, f % 2
    y, c = t // 2, t % 2
    ox, oy, oc = 1 - x, 1 - y, 1 - c
    rows, width = r.tok.shape
    cols = width // nz
    feat = r.upm.shape[0]
    units = r.act.shape[1]
    fine = feat // PIECES
    wide = 2 * fine
    span = 2 * rows
    close = z // 2
    same = (z + 2) % 4
    pair = z + 1 - 2 * (z % 2)
    across = (pair + 2) % 4
    inner, outer = 2 - close, 3 * (1 - close)
    central = jnp.logical_or(z == 1, z == 2)
    at_x = (z * 2 + ox, t)
    at_y = (f, oy * 2 + c)
    at_c = (f, y * 2 + oc)

    def at_z(zz):
        return (zz * 2 + x, t)

    fetch = [pltpu.make_async_copy(src, dst, r.s_in.at[n]) for n, (src, dst) in enumerate(
        ((tok_h, r.tok), (upm_h, r.upm), (dnm_h, r.dnm)))]
    for copy in fetch:
        copy.start()

    barrier = pltpu.get_barrier_semaphore()
    partners = (at_z(pair), at_z(same), at_z(across), at_x, at_y, at_c)
    for dev in partners:
        pl.semaphore_signal(barrier, inc=1, device_id=dev, device_id_type=pl.DeviceIdType.MESH)

    tally = collections.Counter()

    def remote(src, dst, kind, rsem, dev, counted=True):
        if counted:
            tally[kind] += math.prod(src.shape) * jnp.dtype(src.dtype).itemsize
        return pltpu.make_async_remote_copy(
            src_ref=src, dst_ref=dst, send_sem=r.s_out.at[kind], recv_sem=rsem,
            device_id=dev, device_id_type=pl.DeviceIdType.MESH)

    def send(src, dst, kind, rsem, dev):
        remote(src, dst, kind, rsem, dev).start()

    def arrived(dst, rsem):
        remote(dst, dst, 0, rsem, at_x, False).wait_recv()

    def slot(q, zz, xx):
        return (q * nz + zz) * 2 + xx

    def token(q, zz, xx):
        return r.xg.at[slot(q, zz, xx)]

    def blocks_of(n):
        return r.xg.at[pl.ds(0, n)]

    def at_rows(ref, k):
        return ref.at[pl.ds(pl.multiple_of(k * feat, feat), feat), :]

    def at_piece(ref, k, p):
        return ref.at[pl.ds(pl.multiple_of(k * feat + p * fine, fine), fine), :]

    def cast(src, dst, out, factor):
        for m in range(SUB):
            block = src[:, m * units:(m + 1) * units]
            dst[m] = (block if factor is None else factor * block).astype(BF16)
        block = src[:, pl.ds(pl.multiple_of(f * units, units), units)]
        out[pl.ds(pl.multiple_of(f * feat, feat), feat), :] = (
            block if factor is None else factor * block).astype(BF16)

    with mark("norm"):
        fetch[0].wait()
        full = r.tok[...].astype(F32)
        scale = lax.rsqrt(jnp.mean(full * full, axis=1, keepdims=True) + EPS)
        for q in range(nz):
            r.xg[slot(q, z, x)] = (full[:, q * cols:(q + 1) * cols] * scale).astype(BF16)
    with mark("barrier"):
        pl.semaphore_wait(barrier, len(partners))

    TOKEN, WEIGHT, SUM, PASSED = range(4)

    def token_x(zz):
        send(token(t, zz, x), token(t, zz, x), TOKEN, r.r_tx.at[zz], at_x)

    def token_y(zz, xx):
        send(token(t, zz, xx), token(t, zz, xx), TOKEN, r.r_ty.at[zz, xx], at_y)

    def token_c(yy, zz, xx):
        part = token(yy * 2 + c, zz, xx)
        send(part, part, TOKEN, r.r_tc.at[0], at_c)

    def token_in(zz):
        token_x(zz)
        token_y(zz, x)
        token_c(y, zz, x)

    def up_x(zz):
        send(r.up_s.at[zz * 2 + ox], r.up_r.at[zz], WEIGHT, r.r_ux.at[zz], at_x)

    def up_own(zz, far):
        send(r.up_s.at[zz * 2 + x], at_rows(r.up_o, f), WEIGHT, r.r_up.at[far], at_z(zz))

    def up_relay(zz, far):
        arrived(r.up_r.at[zz], r.r_ux.at[zz])
        send(r.up_r.at[zz], at_rows(r.up_o, z * 2 + ox), WEIGHT, r.r_up.at[far], at_z(zz))

    def slab(p):
        return pl.ds(p * fine, fine)

    def dn_x(p):
        for zz in (inner, outer):
            send(r.dn_s.at[zz * 2 + ox, slab(p)], r.dn_r.at[zz, slab(p)], WEIGHT, r.r_dx.at[p], at_x)

    def dn_own(p):
        for zz in (inner, outer):
            send(r.dn_s.at[zz * 2 + x, slab(p)], at_piece(r.dn_o, f, p), WEIGHT, r.r_dl.at[p], at_z(zz))

    def dn_relay(p):
        arrived(r.dn_r.at[pl.ds(0, 2), slab(p)], r.r_dx.at[p])
        for zz in (inner, outer):
            send(r.dn_r.at[zz, slab(p)], at_piece(r.dn_o, z * 2 + ox, p), WEIGHT, r.r_dl.at[p], at_z(zz))

    for to in (inner, pair):
        send(token(t, z, x), token(t, z, x), TOKEN, r.r_tz.at[z], at_z(to))
    token_x(z)
    with mark("castup"):
        fetch[1].wait()
        cast(r.upm, r.up_s, r.up_o, jnp.transpose(gain[...]))
    up_own(pair, 0)
    for zz in (inner, outer):
        up_x(zz)
    for zz in (inner, outer):
        up_own(zz, 1)
    with mark("castdn"):
        fetch[2].wait()
        cast(r.dnm, r.dn_s, r.dn_o, None)
    passed = [
        remote(token(t, zz, x), token(t, zz, x), PASSED, r.r_tz.at[zz], at_z(pair)) for zz in (inner, outer)]
    with mark("tokpair"):
        arrived(token(t, pair, x), r.r_tz.at[pair])
        token_in(pair)
    with mark("toktx0"):
        arrived(token(t, z, ox), r.r_tx.at[z])
        token_y(z, ox)
        token_c(y, z, ox)
    up_x(pair)

    def far_tokens():
        for zz in (inner, outer):
            arrived(token(t, zz, x), r.r_tz.at[zz])

    with mark("tokfarc"):
        @pl.when(central)
        def _():
            far_tokens()
            for copy in passed:
                copy.start()

    with mark("uprelay"):
        for zz in (inner, outer):
            up_relay(zz, 1)
    with mark("tokfare"):
        pl.when(jnp.logical_not(central))(far_tokens)
        for zz in (inner, outer):
            token_in(zz)
    send(r.up_s.at[z * 2 + ox], at_rows(r.up_o, f), WEIGHT, r.r_up.at[0], at_x)
    send(r.dn_s.at[pair * 2 + ox], r.dn_r.at[pair], WEIGHT, r.r_dx.at[PIECES], at_x)
    send(r.dn_s.at[z * 2 + ox], at_rows(r.dn_o, f), WEIGHT, r.r_de.at[0], at_x)
    for p in range(PIECES):
        dn_x(p)
    with mark("uppair"):
        up_relay(pair, 0)
    send(r.dn_s.at[pair * 2 + x], at_rows(r.dn_o, f), WEIGHT, r.r_de.at[0], at_z(pair))
    for zz in (pair, inner, outer):
        with mark("toktx"):
            arrived(token(t, zz, ox), r.r_tx.at[zz])
            token_y(zz, ox)
            token_c(y, zz, ox)
    dn_own(0)
    other = oy * 2 + c
    for zz, xx in ((pair, x), (z, ox), (inner, x), (outer, x), (pair, ox), (inner, ox), (outer, ox)):
        with mark("tokty"):
            arrived(token(other, zz, xx), r.r_ty.at[zz, xx])
            token_c(oy, zz, xx)
    with mark("dnpair"):
        arrived(r.dn_r.at[pair], r.r_dx.at[PIECES])
        send(r.dn_r.at[pair], at_rows(r.dn_o, z * 2 + ox), WEIGHT, r.r_de.at[0], at_z(pair))
    with mark("dnrel0"):
        dn_relay(0)
    with mark("toktc"):
        arrived(blocks_of(2 * (2 * nz - 1)), r.r_tc.at[0])

    def up_dot(q, zz):
        return jnp.dot(r.xg[pl.ds(slot(q, zz, 0), 2)].reshape(span, cols),
                       r.up_o[pl.ds(pl.multiple_of(q * cols, cols), cols), :],
                       preferred_element_type=F32)

    def at_span(zz):
        return pl.ds(pl.multiple_of(zz * span, span), span)

    with mark("upnear"):
        arrived(blocks_of(3), r.r_up.at[0])
    with mark("mmnear"):
        @pl.loop(0, nz)
        def _(zz):
            r.pre[at_span(zz), :] = up_dot(close * 2, zz) + up_dot(close * 2 + 1, zz)
    with mark("dnfar1"):
        dn_own(1)
        dn_relay(1)
    with mark("upfar"):
        arrived(blocks_of(4), r.r_up.at[1])
    with mark("mmfar"):
        @pl.loop(0, nz)
        def _(zz):
            low = (1 - close) * 2
            total = r.pre[at_span(zz), :] + up_dot(low, zz) + up_dot(low + 1, zz)
            r.act[at_span(zz), :] = jnp.square(jnp.maximum(total, 0.0)).astype(BF16)

    mine = (y == close, y != close)
    not_mine = (mine[1], mine[0])
    at_pair, at_same = at_z(pair), at_z(same)

    def block_of(u):
        q, part = UNITS[u]
        if part == "far":
            return q, 2 * (1 - close), 2
        if part == "near":
            return q, 2 * close, 2
        return q, 0, nz

    def product(u):
        q, base, n = block_of(u)
        yy, p = (close if q < PIECES else 1 - close), q % PIECES
        if q == 0:
            arrived(blocks_of(3), r.r_de.at[0])
        elif q >= PIECES and UNITS[u][1] != "near":
            arrived(blocks_of(1), r.r_dl.at[p])
        taken = jnp.concatenate(
            [at_piece(r.dn_o, yy * 4 + cc * 2 + xx, p)[...] for cc in (oc, c) for xx in range(2)], axis=0)
        total = lax.dot_general(
            r.act[pl.ds(pl.multiple_of(base * span, span), n * span), :], taken,
            (((1,), (1,)), ((), ())), preferred_element_type=F32)
        at = pl.ds(base, n)
        r.cs[q, at] = total[:, :wide].astype(BF16).reshape(n, 2, rows, wide)
        r.part[q, at] = total[:, wide:].reshape(n, 2, rows, wide)
        send(r.cs.at[q, at], r.cr.at[q, at], SUM, r.r_c.at[u], at_c)

    def over(base, n, body):
        @pl.loop(0, n)
        def _(i):
            body(base + i)

    def core_sum(u):
        q, base, n = block_of(u)
        at = pl.ds(base, n)
        arrived(r.cr.at[q, at], r.r_c.at[u])
        if q not in Y_FIRST:
            def body(zz):
                r.xb[q, zz] = (r.part[q, zz, ox] + r.cr[q, zz, ox].astype(F32)).astype(BF16)
                r.xs[q, zz] = r.part[q, zz, x] + r.cr[q, zz, x].astype(F32)

            over(base, n, body)
            send(r.xb.at[q, at], r.xr.at[q, at], SUM, r.r_x.at[u], at_x)
        else:
            theirs = not_mine[q // PIECES]
            over_y = remote(r.fb.at[q, at], r.fr.at[q, at], SUM, r.r_y.at[u], at_y, q < PIECES)

            @pl.when(theirs)
            def _():
                def body(zz):
                    r.fb[q, zz] = (r.part[q, zz] + r.cr[q, zz].astype(F32)).astype(BF16)

                over(base, n, body)
                over_y.start()

    def first_sum(u):
        q, base, n = block_of(u)
        at = pl.ds(base, n)
        if q not in Y_FIRST:
            theirs = not_mine[q // PIECES]
            arrived(r.xr.at[q, at], r.r_x.at[u])
            over_y = remote(r.yb.at[q, at], r.yr.at[q, at], SUM, r.r_y.at[u], at_y, q < PIECES)

            @pl.when(theirs)
            def _():
                def body(zz):
                    r.yb[q, zz] = (r.xs[q, zz] + r.xr[q, zz].astype(F32)).astype(BF16)

                over(base, n, body)
                over_y.start()
        else:
            ours = mine[q // PIECES]
            over_x = remote(r.xb.at[q, at], r.xr.at[q, at], SUM, r.r_x.at[u], at_x, q < PIECES)

            @pl.when(ours)
            def _():
                arrived(r.fr.at[q, at], r.r_y.at[u])

                def body(zz):
                    def whole(xx):
                        return (r.part[q, zz, xx] + r.cr[q, zz, xx].astype(F32)
                                + r.fr[q, zz, xx].astype(F32))

                    r.xb[q, zz] = whole(ox).astype(BF16)
                    r.xs[q, zz] = whole(x)

                over(base, n, body)
                over_x.start()

    def second_sum(u):
        q, base, n = block_of(u)
        at, ours, p = pl.ds(base, n), mine[q // PIECES], q % PIECES
        part = UNITS[u][1]
        to_pair = [
            remote(r.zb.at[p, who], r.zr.at[p, m], SUM, r.r_z.at[p, m], at_pair, q < PIECES)
            for m, who in ((0, across), (1, pair)) if part != ("near", "far")[m]]

        @pl.when(ours)
        def _():
            if q in Y_FIRST:
                arrived(r.xr.at[q, at], r.r_x.at[u])
            else:
                arrived(r.yr.at[q, at], r.r_y.at[u])

            def body(zz):
                total = r.xs[q, zz] + r.xr[q, zz].astype(F32)
                if q not in Y_FIRST:
                    total = total + r.yr[q, zz].astype(F32)
                r.kept[p, zz] = total
                r.zb[p, zz] = total.astype(BF16)

            over(base, n, body)
            for copy in to_pair:
                copy.start()

    def cross_sum(u):
        q = UNITS[u][0]
        ours, p = mine[q // PIECES], q % PIECES
        over_z = remote(r.zc.at[p], r.zr.at[p, 2], SUM, r.r_z.at[p, 1], at_same, q < PIECES)

        @pl.when(ours)
        def _():
            arrived(r.zr.at[p, 0], r.r_z.at[p, 0])
            r.zc[p] = (r.kept[p, same] + r.zr[p, 0].astype(F32)).astype(BF16)
            over_z.start()

    def more_down(p):
        dn_own(p)
        dn_relay(p)

    stages = dict(a=product, b=core_sum, c=first_sum, d=second_sum, e=cross_sum, D=more_down)
    for step in ORDER:
        with mark("st_" + step):
            stages[step[0]](int(step[1]))
    for p in range(PIECES):
        with mark("final%d" % p):
            arrived(r.zr.at[p, pl.ds(1, 2)], r.r_z.at[p, 1])
            total = (r.kept[p, z] + r.zr[p, 1].astype(F32) + r.zr[p, 2].astype(F32)).astype(BF16)
            for xx in range(2):
                mix_o[:, xx * feat + p * fine:xx * feat + (p + 1) * fine] = total[:, xx * fine:(xx + 1) * fine]
    with mark("drain"):
        block = rows * cols * jnp.dtype(BF16).itemsize

        def wait_sent(kind):
            assert tally[kind] % block == 0
            done = blocks_of(tally[kind] // block)
            remote(done, done, kind, r.r_tc.at[0], at_x, False).wait_send()

        for kind in (TOKEN, WEIGHT, SUM):
            wait_sent(kind)
        pl.when(central)(lambda: wait_sent(PASSED))


UNITS = tuple((q, "all") for q in range(7)) + ((7, "far"), (7, "near"))
Y_FIRST = (0, 4)
ORDER = (
    "a0", "a1", "b0", "a2", "b1", "a3", "b2", "b3", "D2", "a4", "b4", "D3", "c1", "c2", "c0", "a5", "b5",
    "c3", "d1", "c4", "d2", "d0", "a6", "b6", "c5", "d3", "d4", "a7", "a8", "b7", "b8", "c6", "e1", "e2", "e0", "e3",
    "d5", "e4", "c7", "c8", "d6", "e5", "d7", "e6", "d8", "e7",
)


def on_device_fused(tokens, gain, up_master, down_master):
    rows, width = tokens.shape
    feat, ff = up_master.shape
    units = ff // SUB
    nz = SUB // 2
    cols = width // nz
    fine = feat // PIECES
    wide = 2 * fine
    n, pieces = len(UNITS), 2 * PIECES
    dma = pltpu.SemaphoreType.DMA
    vmem = pl.BlockSpec(memory_space=pltpu.VMEM)
    hbm = pl.BlockSpec(memory_space=pltpu.HBM)
    anywhere = pl.BlockSpec(memory_space=pl.ANY)
    arrays = dict(
        tok=((rows, width), BF16), upm=((feat, ff), F32), dnm=((feat, ff), F32),
        xg=((2 * nz * nz, rows, cols), BF16),
        up_s=((SUB, feat, units), BF16), dn_s=((SUB, feat, units), BF16),
        up_r=((nz, feat, units), BF16), dn_r=((nz, feat, units), BF16),
        pre=((SUB * rows, units), F32), act=((SUB * rows, units), BF16),
        cs=((pieces, nz, 2, rows, wide), BF16), cr=((pieces, nz, 2, rows, wide), BF16),
        part=((pieces, nz, 2, rows, wide), F32),
        xs=((pieces, nz, rows, wide), F32), xb=((pieces, nz, rows, wide), BF16), xr=((pieces, nz, rows, wide), BF16),
        yb=((pieces, nz, rows, wide), BF16), yr=((pieces, nz, rows, wide), BF16),
        fb=((pieces, nz, 2, rows, wide), BF16), fr=((pieces, nz, 2, rows, wide), BF16),
        kept=((PIECES, nz, rows, wide), F32), zb=((PIECES, nz, rows, wide), BF16),
        zc=((PIECES, rows, wide), BF16), zr=((PIECES, 3, rows, wide), BF16),
    )
    sems = dict(
        s_in=(3,), s_out=(4,), r_tz=(nz,), r_tx=(nz,), r_ty=(nz, 2), r_tc=(1,), r_ux=(nz,), r_up=(2,),
        r_dx=(PIECES + 1,), r_de=(1,), r_dl=(PIECES,), r_c=(n,), r_x=(n,), r_y=(n,), r_z=(PIECES, 2),
    )
    names = list(arrays) + list(sems)
    up_s, dn_s, mixed = pl.pallas_call(
        functools.partial(fused, nz, names),
        out_shape=(
            pltpu.VMEM((SUB * feat, units), BF16),
            pltpu.VMEM((SUB * feat, units), BF16),
            pltpu.VMEM((rows, cols), BF16),
        ),
        in_specs=[hbm, vmem, hbm, hbm],
        out_specs=(vmem, vmem, vmem),
        scratch_shapes=[pltpu.VMEM(*spec) for spec in arrays.values()] + [dma(shape) for shape in sems.values()],
        compiler_params=pltpu.CompilerParams(
            collective_id=0, has_side_effects=True, vmem_limit_bytes=62873 * 2**10),
    )(tokens, gain[None, :], up_master, down_master)
    shapes = [jax.ShapeDtypeStruct(a.shape, a.dtype) for a in (up_s, dn_s, mixed)]
    up_s, dn_s, mixed = pl.pallas_call(
        write_out, out_shape=shapes, in_specs=[anywhere] * 3, out_specs=[anywhere] * 3,
        scratch_shapes=[dma((3,))],
        compiler_params=pltpu.CompilerParams(vmem_limit_bytes=2**20),
    )(up_s, dn_s, mixed)
    return up_s[None], dn_s[None], mixed


def write_out(*refs):
    copies = [pltpu.make_async_copy(refs[n], refs[3 + n], refs[6].at[n]) for n in range(3)]
    for copy in copies:
        copy.start()
    for copy in copies:
        copy.wait()


def from_partner(block, axis, bit):
    count = lax.axis_size(axis)
    route = []
    for low in range(count):
        high = low | 1 << bit
        if high != low and high < count:
            route += [(low, high), (high, low)]
    return lax.ppermute(block, axis, route)


def on_device(tokens, gain, up_master, down_master):
    fs_count = lax.axis_size("fs")
    feat_rows = up_master.shape[0]
    units = up_master.shape[1] // SUB
    groups_count = fs_count // SUB
    member = lax.axis_index("fs") % SUB
    up_round = (gain[:, None] * up_master).astype(jnp.bfloat16)
    down_round = down_master.astype(jnp.bfloat16)

    def spread(weight):
        blocks = weight.reshape(feat_rows, SUB, units).transpose(1, 0, 2)
        return jnp.broadcast_to(blocks[None], (groups_count, SUB, feat_rows, units)).reshape(
            fs_count, feat_rows, units
        )

    up_sampled, down_sampled = (
        lax.all_to_all(spread(up_round), "fs", split_axis=0, concat_axis=1, tiled=True),
        lax.all_to_all(spread(down_round), "fs", split_axis=0, concat_axis=1, tiled=True),
    )
    levels = SUB.bit_length() - 1
    bit_list = list(range(levels))
    widened = tokens.astype(jnp.float32)
    normed = (
        widened * lax.rsqrt(jnp.mean(widened * widened, axis=1, keepdims=True) + 1e-06)
    ).astype(jnp.bfloat16)
    current = normed[None]
    for bit in bit_list:
        partner = from_partner(current, "fs", bit)
        lower = member >> bit & 1 == 0
        current = jnp.where(lower, jnp.stack([current, partner]), jnp.stack([partner, current]))
    order_now = list(reversed(bit_list))
    wanted = list(range(levels - 1, -1, -1))
    perm_axes = [
        [place for place, value in enumerate(order_now) if value == target][0] for target in wanted
    ]
    current = jnp.transpose(current, perm_axes + [levels, levels + 1, levels + 2])
    gathered = current.reshape(SUB * tokens.shape[0], tokens.shape[1])
    pre_units = jnp.dot(gathered, up_sampled[0], preferred_element_type=jnp.float32)
    act_units = jnp.square(jax.nn.relu(pre_units)).astype(jnp.bfloat16)
    partial_out = lax.dot_general(
        act_units, down_sampled[0], (((1,), (1,)), ((), ())), preferred_element_type=jnp.float32
    )
    running = partial_out.reshape((2,) * levels + (tokens.shape[0], tokens.shape[1]))
    axis_bits = list(range(levels - 1, -1, -1))
    for bit in bit_list:
        position = len([value for value in axis_bits if value > bit])
        mine = member >> bit & 1
        keep = lax.dynamic_index_in_dim(running, mine, position, keepdims=False)
        other = lax.dynamic_index_in_dim(running, 1 - mine, position, keepdims=False)
        running = keep + from_partner(other, "fs", bit)
        axis_bits = [value for value in axis_bits if value != bit]
    summed = lax.psum_scatter(running, "tp", scatter_dimension=1, tiled=True)
    return (up_sampled, down_sampled, summed.astype(jnp.bfloat16))


def solution(mesh):
    placed = (P("fs", None), P("fs"), P("fs", "tp"), P("fs", "tp"))
    one_group = mesh.shape["fs"] == SUB and mesh.shape["tp"] == 4
    return jax.shard_map(
        on_device_fused if one_group else on_device,
        mesh=mesh,
        in_specs=placed,
        out_specs=(P("fs", None, "tp"), P("fs", None, "tp"), P("fs", "tp")),
        check_vma=False,
    )
```

time: 88.1 us -> 80.5 us (0.914)
  local copies, waits for them, and re-layouts: 3.99 us -> 0 us
  Pallas kernels: 83.3 us -> 79.7 us
    unnamed x7 -> x0, local copies, waits for them, and re-layouts: 3.99 us -> none
    pallas_call x1 -> x2, Pallas kernels: 83.3 us -> 79.7 us  [the longest x1 78.3 us: on_device_fused(): pl.pallas_call(functools.partial(fused, nz, names), out_shape=(pltpu.VMEM...]
where the time goes in v2:
time: 80.5 us; the launch traced here: 80.3 us
  Pallas kernels  79.7 us (99%)
    pallas_call x1, Pallas kernels, on_device_fused(): pl.pallas_call(functools.partial(fused, nz, names), out_shape=(pltpu.VMEM...  78.3 us

profile of v2, /device:TPU:0, one launch (start us, length us, event | category | flops | bytes accessed | tf_op | source)
XLA Modules:
  0.0 80.3 jit_solution(3136573859526568279)
XLA Ops:
  0.6 78.3 %shard_map.67 = (bf16[2048,256]{1,0:T(8,128)(2,1)S(1)}, bf16[2048,256]{1,0:T(8,128)(2,1)S(1)}, bf16[128,512]{1,0:T(8,128)(2,1)S(1)}) custom-call(bf16[128,2048]{1,0:T(8,128)(2,1)} %tok_h.1, f32[1,256]{1,0:T(1,128)} %bitcast.3, f32[256,2048]{1,0:T(8,128)} %upm_h.1, f32[256,2048]{1,0:T(8,128)} %dnm_h.1), custom_call_target="tpu_custom_call" | custom-call | tf_op jit(solution)/shard_map/pallas_call | solution.py:440
  78.9 1.4 %shard_map.68 = (bf16[2048,256]{1,0:T(8,128)(2,1)}, bf16[2048,256]{1,0:T(8,128)(2,1)}, bf16[128,512]{1,0:T(8,128)(2,1)}) custom-call(bf16[2048,256]{1,0:T(8,128)(2,1)S(1)} %get-tuple-element.9.refs_0_, bf16[2048,256]{1,0:T(8,128)(2,1)S(1)} %get-tuple-element.10.refs_1_, bf16[128,512]{1,0:T(8,128)(2,1)S(1)} %get-tuple-element.11.refs_2_), custom_call_target="tpu_custom_call" | custom-call | tf_op jit(solution)/shard_map/pallas_call | solution.py:454

commit v3 on v2

--- a/solution.py
+++ b/solution.py
@@ -30,7 +30,7 @@
     feat = r.upm.shape[0]
     units = r.act.shape[1]
     fine = feat // PIECES
-    wide = 2 * fine
+    wide, half_wide = 4 * fine, 2 * fine
     span = 2 * rows
     close = z // 2
     same = (z + 2) % 4
@@ -51,9 +51,16 @@
         copy.start()
 
     barrier = pltpu.get_barrier_semaphore()
-    partners = (at_z(pair), at_z(same), at_z(across), at_x, at_y, at_c)
-    for dev in partners:
+    def greet(dev):
         pl.semaphore_signal(barrier, inc=1, device_id=dev, device_id_type=pl.DeviceIdType.MESH)
+
+    for dev in (at_z(pair), at_x, at_y, at_c):
+        greet(dev)
+
+    @pl.when(central)
+    def _():
+        greet(at_z(inner))
+        greet(at_z(outer))
 
     tally = collections.Counter()
 
@@ -100,30 +107,51 @@
         for q in range(nz):
             r.xg[slot(q, z, x)] = (full[:, q * cols:(q + 1) * cols] * scale).astype(BF16)
     with mark("barrier"):
-        pl.semaphore_wait(barrier, len(partners))
-
-    TOKEN, WEIGHT, SUM, PASSED = range(4)
-
-    def token_x(zz):
-        send(token(t, zz, x), token(t, zz, x), TOKEN, r.r_tx.at[zz], at_x)
-
-    def token_y(zz, xx):
-        send(token(t, zz, xx), token(t, zz, xx), TOKEN, r.r_ty.at[zz, xx], at_y)
-
-    def token_c(yy, zz, xx):
-        part = token(yy * 2 + c, zz, xx)
-        send(part, part, TOKEN, r.r_tc.at[0], at_c)
-
-    def token_in(zz):
-        token_x(zz)
-        token_y(zz, x)
-        token_c(y, zz, x)
+        pl.semaphore_wait(barrier, 5)
+
+    TOKEN, WEIGHT, SUM, PASSED, OURS, THEIRS = range(6)
+
+    def hop(q, zz, xx, rsem, dev, kind=TOKEN):
+        return remote(token(q, zz, xx), token(q, zz, xx), kind, rsem, dev)
+
+    other = oy * 2 + c
+    at = dict(own=z, pair=pair, inner=inner, outer=outer)
+    at_xx = dict(x=x, ox=ox)
+    over_x = {w: hop(t, zz, x, r.r_tx.at[zz], at_x) for w, zz in at.items()}
+    places = [(w, xx) for w in at for xx in at_xx if (w, xx) != ("own", "x")]
+    over_y = {(w, xx): hop(t, at[w], at_xx[xx], r.r_ty.at[at[w], at_xx[xx]], at_y) for w, xx in places}
+    over_c = {(n, w, xx): hop(q, at[w], at_xx[xx], r.r_tc.at[0], at_c)
+              for n, q in enumerate((t, other)) for w, xx in places}
+    passed = {w: hop(t, at[w], x, r.r_tz.at[at[w]], at_z(pair), PASSED) for w in ("inner", "outer")}
+
+    def spread(w, xx):
+        over_y[w, xx].start()
+        over_c[0, w, xx].start()
+
+    def from_z(w, relayed=False):
+        arrived(token(t, at[w], x), r.r_tz.at[at[w]])
+        if relayed:
+            passed[w].start()
+        over_x[w].start()
+        spread(w, "x")
+
+    def from_x(w):
+        arrived(token(t, at[w], ox), r.r_tx.at[at[w]])
+        spread(w, "ox")
+
+    def from_y(w, xx):
+        arrived(token(other, at[w], at_xx[xx]), r.r_ty.at[at[w], at_xx[xx]])
+        over_c[1, w, xx].start()
+
+    def either(when_central, when_end):
+        pl.when(central)(when_central)
+        pl.when(jnp.logical_not(central))(when_end)
 
     def up_x(zz):
         send(r.up_s.at[zz * 2 + ox], r.up_r.at[zz], WEIGHT, r.r_ux.at[zz], at_x)
 
-    def up_own(zz, far):
-        send(r.up_s.at[zz * 2 + x], at_rows(r.up_o, f), WEIGHT, r.r_up.at[far], at_z(zz))
+    def up_own(zz, far, counted=True):
+        remote(r.up_s.at[zz * 2 + x], at_rows(r.up_o, f), WEIGHT, r.r_up.at[far], at_z(zz), counted).start()
 
     def up_relay(zz, far):
         arrived(r.up_r.at[zz], r.r_ux.at[zz])
@@ -146,72 +174,100 @@
             send(r.dn_r.at[zz, slab(p)], at_piece(r.dn_o, z * 2 + ox, p), WEIGHT, r.r_dl.at[p], at_z(zz))
 
     for to in (inner, pair):
-        send(token(t, z, x), token(t, z, x), TOKEN, r.r_tz.at[z], at_z(to))
-    token_x(z)
+        hop(t, z, x, r.r_tz.at[z], at_z(to)).start()
+    over_x["own"].start()
     with mark("castup"):
         fetch[1].wait()
         cast(r.upm, r.up_s, r.up_o, jnp.transpose(gain[...]))
     up_own(pair, 0)
-    for zz in (inner, outer):
-        up_x(zz)
-    for zz in (inner, outer):
-        up_own(zz, 1)
+    up_x(pair)
+    up_x(inner)
+    up_own(inner, 1)
     with mark("castdn"):
         fetch[2].wait()
         cast(r.dnm, r.dn_s, r.dn_o, None)
-    passed = [
-        remote(token(t, zz, x), token(t, zz, x), PASSED, r.r_tz.at[zz], at_z(pair)) for zz in (inner, outer)]
-    with mark("tokpair"):
-        arrived(token(t, pair, x), r.r_tz.at[pair])
-        token_in(pair)
-    with mark("toktx0"):
-        arrived(token(t, z, ox), r.r_tx.at[z])
-        token_y(z, ox)
-        token_c(y, z, ox)
-    up_x(pair)
-
-    def far_tokens():
-        for zz in (inner, outer):
-            arrived(token(t, zz, x), r.r_tz.at[zz])
-
-    with mark("tokfarc"):
-        @pl.when(central)
-        def _():
-            far_tokens()
-            for copy in passed:
-                copy.start()
-
+
+    def central_first():
+        with mark("cinner"):
+            from_z("inner", True)
+        with mark("couter"):
+            from_z("outer", True)
+
+    def end_first():
+        with mark("epair"):
+            from_z("pair")
+        with mark("exz"):
+            from_x("own")
+
+    either(central_first, end_first)
+    up_x(outer)
+
+    def central_second():
+        with mark("cpair"):
+            from_z("pair")
+        with mark("cxz"):
+            from_x("own")
+
+    pl.when(central)(central_second)
+    with mark("uppair"):
+        up_relay(pair, 0)
+    send(r.dn_s.at[pair * 2 + x], at_rows(r.dn_o, f), WEIGHT, r.r_de.at[0], at_z(pair))
     with mark("uprelay"):
-        for zz in (inner, outer):
-            up_relay(zz, 1)
-    with mark("tokfare"):
-        pl.when(jnp.logical_not(central))(far_tokens)
-        for zz in (inner, outer):
-            token_in(zz)
+        up_relay(inner, 1)
+
+    def central_third():
+        up_own(outer, 1)
+        with mark("cxinner"):
+            from_x("inner")
+        with mark("cxouter"):
+            from_x("outer")
+
+    def end_third():
+        with mark("expair"):
+            from_x("pair")
+        with mark("einner"):
+            from_z("inner")
+        with mark("eouter"):
+            from_z("outer")
+        up_own(outer, 1, False)
+
+    either(central_third, end_third)
+    send(r.dn_s.at[pair * 2 + ox], r.dn_r.at[pair], WEIGHT, r.r_dx.at[PIECES], at_x)
     send(r.up_s.at[z * 2 + ox], at_rows(r.up_o, f), WEIGHT, r.r_up.at[0], at_x)
-    send(r.dn_s.at[pair * 2 + ox], r.dn_r.at[pair], WEIGHT, r.r_dx.at[PIECES], at_x)
     send(r.dn_s.at[z * 2 + ox], at_rows(r.dn_o, f), WEIGHT, r.r_de.at[0], at_x)
     for p in range(PIECES):
         dn_x(p)
-    with mark("uppair"):
-        up_relay(pair, 0)
-    send(r.dn_s.at[pair * 2 + x], at_rows(r.dn_o, f), WEIGHT, r.r_de.at[0], at_z(pair))
-    for zz in (pair, inner, outer):
-        with mark("toktx"):
-            arrived(token(t, zz, ox), r.r_tx.at[zz])
-            token_y(zz, ox)
-            token_c(y, zz, ox)
+    with mark("uprelay"):
+        up_relay(outer, 1)
     dn_own(0)
-    other = oy * 2 + c
-    for zz, xx in ((pair, x), (z, ox), (inner, x), (outer, x), (pair, ox), (inner, ox), (outer, ox)):
-        with mark("tokty"):
-            arrived(token(other, zz, xx), r.r_ty.at[zz, xx])
-            token_c(oy, zz, xx)
+
+    def central_fourth():
+        with mark("cxpair"):
+            from_x("pair")
+
+    def end_fourth():
+        with mark("exinner"):
+            from_x("inner")
+        with mark("exouter"):
+            from_x("outer")
+
+    def central_fifth():
+        with mark("cy"):
+            for w, xx in (("inner", "x"), ("outer", "x"), ("pair", "x"), ("own", "ox"),
+                          ("inner", "ox"), ("outer", "ox"), ("pair", "ox")):
+                from_y(w, xx)
+
+    def end_fifth():
+        with mark("ey"):
+            for w, xx in (("pair", "x"), ("own", "ox"), ("pair", "ox"), ("inner", "x"),
+                          ("outer", "x"), ("inner", "ox"), ("outer", "ox")):
+                from_y(w, xx)
+
+    either(central_fourth, end_fourth)
     with mark("dnpair"):
         arrived(r.dn_r.at[pair], r.r_dx.at[PIECES])
         send(r.dn_r.at[pair], at_rows(r.dn_o, z * 2 + ox), WEIGHT, r.r_de.at[0], at_z(pair))
-    with mark("dnrel0"):
-        dn_relay(0)
+    either(central_fifth, end_fifth)
     with mark("toktc"):
         arrived(blocks_of(2 * (2 * nz - 1)), r.r_tc.at[0])
 
@@ -229,9 +285,8 @@
         @pl.loop(0, nz)
         def _(zz):
             r.pre[at_span(zz), :] = up_dot(close * 2, zz) + up_dot(close * 2 + 1, zz)
-    with mark("dnfar1"):
-        dn_own(1)
-        dn_relay(1)
+    with mark("dnrel0"):
+        dn_relay(0)
     with mark("upfar"):
         arrived(blocks_of(4), r.r_up.at[1])
     with mark("mmfar"):
@@ -241,167 +296,204 @@
             total = r.pre[at_span(zz), :] + up_dot(low, zz) + up_dot(low + 1, zz)
             r.act[at_span(zz), :] = jnp.square(jnp.maximum(total, 0.0)).astype(BF16)
 
-    mine = (y == close, y != close)
-    not_mine = (mine[1], mine[0])
     at_pair, at_same = at_z(pair), at_z(same)
-
-    def block_of(u):
-        q, part = UNITS[u]
+    my_half = (1 - c) * close + c * (1 - close)
+    ours, theirs = y == my_half, y != my_half
+    first_core = c == 0
+
+    def block_of(kind, u):
+        j, part = UNITS[kind][u]
         if part == "far":
-            return q, 2 * (1 - close), 2
+            return j, 2 * (1 - close), 2
         if part == "near":
-            return q, 2 * close, 2
-        return q, 0, nz
-
-    def product(u):
-        q, base, n = block_of(u)
-        yy, p = (close if q < PIECES else 1 - close), q % PIECES
-        if q == 0:
-            arrived(blocks_of(3), r.r_de.at[0])
-        elif q >= PIECES and UNITS[u][1] != "near":
-            arrived(blocks_of(1), r.r_dl.at[p])
+            return j, 2 * close, 2
+        return j, 0, nz
+
+    def product(kind, u):
+        j, base, n = block_of(kind, u)
+        half = close if kind == "E" else 1 - close
+        need = ("E", 0) if kind == "E" else ("L", j)
+        if need not in seen:
+            seen.add(need)
+            arrived(blocks_of(3) if kind == "E" else blocks_of(1), r.r_de.at[0] if kind == "E" else r.r_dl.at[j])
         taken = jnp.concatenate(
-            [at_piece(r.dn_o, yy * 4 + cc * 2 + xx, p)[...] for cc in (oc, c) for xx in range(2)], axis=0)
+            [at_piece(r.dn_o, half * 4 + m, j)[...] for m in range(4)], axis=0)
         total = lax.dot_general(
             r.act[pl.ds(pl.multiple_of(base * span, span), n * span), :], taken,
-            (((1,), (1,)), ((), ())), preferred_element_type=F32)
-        at = pl.ds(base, n)
-        r.cs[q, at] = total[:, :wide].astype(BF16).reshape(n, 2, rows, wide)
-        r.part[q, at] = total[:, wide:].reshape(n, 2, rows, wide)
-        send(r.cs.at[q, at], r.cr.at[q, at], SUM, r.r_c.at[u], at_c)
+            (((1,), (1,)), ((), ())), preferred_element_type=F32).reshape(n, 2, rows, wide)
+        here = pl.ds(base, n)
+        if (kind == "E") == (now_core == 0):
+            r.part[j, here] = total
+        else:
+            r.cs[j, here] = total.astype(BF16)
+            send(r.cs.at[j, here], r.cr.at[j, here], SUM, r.r_c.at[u], at_c)
 
     def over(base, n, body):
         @pl.loop(0, n)
         def _(i):
             body(base + i)
 
-    def core_sum(u):
-        q, base, n = block_of(u)
-        at = pl.ds(base, n)
-        arrived(r.cr.at[q, at], r.r_c.at[u])
-        if q not in Y_FIRST:
+    def core_sum(kind, u):
+        j, base, n = block_of(kind, u)
+        here = pl.ds(base, n)
+        arrived(r.cr.at[j, here], r.r_c.at[u])
+        if j not in Y_FIRST[kind]:
             def body(zz):
-                r.xb[q, zz] = (r.part[q, zz, ox] + r.cr[q, zz, ox].astype(F32)).astype(BF16)
-                r.xs[q, zz] = r.part[q, zz, x] + r.cr[q, zz, x].astype(F32)
+                r.xb[j, zz] = (r.part[j, zz, ox] + r.cr[j, zz, ox].astype(F32)).astype(BF16)
+                r.xs[j, zz] = r.part[j, zz, x] + r.cr[j, zz, x].astype(F32)
 
             over(base, n, body)
-            send(r.xb.at[q, at], r.xr.at[q, at], SUM, r.r_x.at[u], at_x)
+            send(r.xb.at[j, here], r.xr.at[j, here], SUM, r.r_x.at[u], at_x)
         else:
-            theirs = not_mine[q // PIECES]
-            over_y = remote(r.fb.at[q, at], r.fr.at[q, at], SUM, r.r_y.at[u], at_y, q < PIECES)
-
             @pl.when(theirs)
             def _():
                 def body(zz):
-                    r.fb[q, zz] = (r.part[q, zz] + r.cr[q, zz].astype(F32)).astype(BF16)
+                    r.fb[j, zz] = (r.part[j, zz] + r.cr[j, zz].astype(F32)).astype(BF16)
 
                 over(base, n, body)
-                over_y.start()
-
-    def first_sum(u):
-        q, base, n = block_of(u)
-        at = pl.ds(base, n)
-        if q not in Y_FIRST:
-            theirs = not_mine[q // PIECES]
-            arrived(r.xr.at[q, at], r.r_x.at[u])
-            over_y = remote(r.yb.at[q, at], r.yr.at[q, at], SUM, r.r_y.at[u], at_y, q < PIECES)
+                send(r.fb.at[j, here], r.fr.at[j, here], THEIRS, r.r_y.at[u], at_y)
+
+    def first_sum(kind, u):
+        j, base, n = block_of(kind, u)
+        here = pl.ds(base, n)
+        if j not in Y_FIRST[kind]:
+            arrived(r.xr.at[j, here], r.r_x.at[u])
 
             @pl.when(theirs)
             def _():
                 def body(zz):
-                    r.yb[q, zz] = (r.xs[q, zz] + r.xr[q, zz].astype(F32)).astype(BF16)
+                    r.yb[j, zz] = (r.xs[j, zz] + r.xr[j, zz].astype(F32)).astype(BF16)
 
                 over(base, n, body)
-                over_y.start()
+                send(r.yb.at[j, here], r.yr.at[j, here], THEIRS, r.r_y.at[u], at_y)
         else:
-            ours = mine[q // PIECES]
-            over_x = remote(r.xb.at[q, at], r.xr.at[q, at], SUM, r.r_x.at[u], at_x, q < PIECES)
-
             @pl.when(ours)
             def _():
-                arrived(r.fr.at[q, at], r.r_y.at[u])
+                arrived(r.fr.at[j, here], r.r_y.at[u])
 
                 def body(zz):
                     def whole(xx):
-                        return (r.part[q, zz, xx] + r.cr[q, zz, xx].astype(F32)
-                                + r.fr[q, zz, xx].astype(F32))
-
-                    r.xb[q, zz] = whole(ox).astype(BF16)
-                    r.xs[q, zz] = whole(x)
+                        return (r.part[j, zz, xx] + r.cr[j, zz, xx].astype(F32)
+                                + r.fr[j, zz, xx].astype(F32))
+
+                    r.xb[j, zz] = whole(ox).astype(BF16)
+                    r.xs[j, zz] = whole(x)
 
                 over(base, n, body)
-                over_x.start()
-
-    def second_sum(u):
-        q, base, n = block_of(u)
-        at, ours, p = pl.ds(base, n), mine[q // PIECES], q % PIECES
-        part = UNITS[u][1]
-        to_pair = [
-            remote(r.zb.at[p, who], r.zr.at[p, m], SUM, r.r_z.at[p, m], at_pair, q < PIECES)
-            for m, who in ((0, across), (1, pair)) if part != ("near", "far")[m]]
+                send(r.xb.at[j, here], r.xr.at[j, here], OURS, r.r_x.at[u], at_x)
+
+    def second_sum(kind, u):
+        j, base, n = block_of(kind, u)
+        here, part = pl.ds(base, n), UNITS[kind][u][1]
 
         @pl.when(ours)
         def _():
-            if q in Y_FIRST:
-                arrived(r.xr.at[q, at], r.r_x.at[u])
+            if j in Y_FIRST[kind]:
+                arrived(r.xr.at[j, here], r.r_x.at[u])
             else:
-                arrived(r.yr.at[q, at], r.r_y.at[u])
+                arrived(r.yr.at[j, here], r.r_y.at[u])
 
             def body(zz):
-                total = r.xs[q, zz] + r.xr[q, zz].astype(F32)
-                if q not in Y_FIRST:
-                    total = total + r.yr[q, zz].astype(F32)
-                r.kept[p, zz] = total
-                r.zb[p, zz] = total.astype(BF16)
+                total = r.xs[j, zz] + r.xr[j, zz].astype(F32)
+                if j not in Y_FIRST[kind]:
+                    total = total + r.yr[j, zz].astype(F32)
+                r.kept[j, zz] = total
+                r.zb[j, zz] = total.astype(BF16)
 
             over(base, n, body)
-            for copy in to_pair:
-                copy.start()
-
-    def cross_sum(u):
-        q = UNITS[u][0]
-        ours, p = mine[q // PIECES], q % PIECES
-        over_z = remote(r.zc.at[p], r.zr.at[p, 2], SUM, r.r_z.at[p, 1], at_same, q < PIECES)
+            for m, who in ((0, across), (1, pair)):
+                if part != ("near", "far")[m]:
+                    send(r.zb.at[j, who], r.zr.at[j, m], OURS, r.r_z.at[j, m], at_pair)
+
+    def cross_sum(kind, u):
+        j = UNITS[kind][u][0]
 
         @pl.when(ours)
         def _():
-            arrived(r.zr.at[p, 0], r.r_z.at[p, 0])
-            r.zc[p] = (r.kept[p, same] + r.zr[p, 0].astype(F32)).astype(BF16)
-            over_z.start()
-
-    def more_down(p):
+            arrived(r.zr.at[j, 0], r.r_z.at[j, 0])
+            total = (r.kept[j, same] + r.zr[j, 0].astype(F32)).astype(BF16)
+            for cc in range(2):
+                r.zc[j, cc] = total[:, cc * half_wide:(cc + 1) * half_wide]
+                send(r.zc.at[j, cc], r.zx.at[j], OURS, r.r_zx.at[j], (same * 2 + x, y * 2 + cc))
+
+    def near_sum(kind, u):
+        j = UNITS[kind][u][0]
+
+        @pl.when(ours)
+        def _():
+            arrived(r.zr.at[j, 1], r.r_z.at[j, 1])
+            total = r.kept[j, z] + r.zr[j, 1].astype(F32)
+            mine = 0 if kind == "E" else 1
+            r.ho[j] = total[:, (1 - mine) * half_wide:(2 - mine) * half_wide]
+            send(r.ho.at[j], r.hi.at[j], OURS, r.r_h.at[j], at_c)
+            r.own[j] = total[:, mine * half_wide:(mine + 1) * half_wide]
+
+    def last_sum(kind, j):
+
+        def put(base):
+            total = (base + r.zx[j].astype(F32)).astype(BF16)
+            for xx in range(2):
+                mix_o[:, xx * feat + j * fine:xx * feat + (j + 1) * fine] = total[:, xx * fine:(xx + 1) * fine]
+
+        arrived(r.zx.at[j], r.r_zx.at[j])
+        pl.when(ours)(lambda: put(r.own[j]))
+
+        @pl.when(theirs)
+        def _():
+            arrived(r.hi.at[j], r.r_h.at[j])
+            put(r.hi[j])
+
+    def more_down(kind, p):
         dn_own(p)
         dn_relay(p)
 
-    stages = dict(a=product, b=core_sum, c=first_sum, d=second_sum, e=cross_sum, D=more_down)
-    for step in ORDER:
-        with mark("st_" + step):
-            stages[step[0]](int(step[1]))
-    for p in range(PIECES):
-        with mark("final%d" % p):
-            arrived(r.zr.at[p, pl.ds(1, 2)], r.r_z.at[p, 1])
-            total = (r.kept[p, z] + r.zr[p, 1].astype(F32) + r.zr[p, 2].astype(F32)).astype(BF16)
-            for xx in range(2):
-                mix_o[:, xx * feat + p * fine:xx * feat + (p + 1) * fine] = total[:, xx * fine:(xx + 1) * fine]
-    with mark("drain"):
-        block = rows * cols * jnp.dtype(BF16).itemsize
-
-        def wait_sent(kind):
-            assert tally[kind] % block == 0
-            done = blocks_of(tally[kind] // block)
-            remote(done, done, kind, r.r_tc.at[0], at_x, False).wait_send()
-
-        for kind in (TOKEN, WEIGHT, SUM):
-            wait_sent(kind)
-        pl.when(central)(lambda: wait_sent(PASSED))
-
-
-UNITS = tuple((q, "all") for q in range(7)) + ((7, "far"), (7, "near"))
-Y_FIRST = (0, 4)
+    stages = dict(
+        a=product, b=core_sum, c=first_sum, d=second_sum, e=cross_sum, n=near_sum, f=last_sum, D=more_down)
+
+    seen = set()
+
+    def program(core):
+        seen.clear()
+        for step in ORDER[core]:
+            with mark(step):
+                stages[step[0]](step[1], int(step[2]))
+
+    def wait_sent(kind):
+        lines = tally[kind] // (cols * jnp.dtype(BF16).itemsize)
+        count, deep = next((lines // deep, deep) for deep in range(rows, 0, -16) if lines % deep == 0)
+        done = r.xg.at[pl.ds(0, count), pl.ds(0, deep)]
+        remote(done, done, kind, r.r_tc.at[0], at_x, False).wait_send()
+
+    def run(core):
+        before = dict(tally)
+        program(core)
+        with mark("drain"):
+            for kind in (TOKEN, WEIGHT, SUM):
+                wait_sent(kind)
+            pl.when(central)(lambda: wait_sent(PASSED))
+            pl.when(ours)(lambda: wait_sent(OURS))
+            pl.when(theirs)(lambda: wait_sent(THEIRS))
+        tally.clear()
+        tally.update(before)
+
+    now_core = 0
+    pl.when(first_core)(lambda: run(0))
+    now_core = 1
+    pl.when(jnp.logical_not(first_core))(lambda: run(1))
+
+
+UNITS = {
+    "E": tuple((j, "all") for j in range(PIECES)),
+    "L": tuple((j, "all") for j in range(PIECES - 1)) + ((PIECES - 1, "far"), (PIECES - 1, "near")),
+}
+Y_FIRST = {"E": (0,), "L": (0,)}
 ORDER = (
-    "a0", "a1", "b0", "a2", "b1", "a3", "b2", "b3", "D2", "a4", "b4", "D3", "c1", "c2", "c0", "a5", "b5",
-    "c3", "d1", "c4", "d2", "d0", "a6", "b6", "c5", "d3", "d4", "a7", "a8", "b7", "b8", "c6", "e1", "e2", "e0", "e3",
-    "d5", "e4", "c7", "c8", "d6", "e5", "d7", "e6", "d8", "e7",
+    ("DE1", "aE0", "aE1", "bE0", "aE2", "bE1", "aE3", "bE2", "DE2", "aL0", "bE3", "aL1", "DE3", "cE1", "cE0",
+     "cE2", "aL2", "dE1", "cE3", "aL3", "aL4", "dE2", "dE0", "dE3", "eE1", "eE2", "eE0", "eE3", "nE1", "nE2",
+     "nE0", "nE3", "fE0", "fE1", "fE2", "fE3"),
+    ("DL1", "aE0", "aE1", "aE2", "aE3", "aL0", "bL0", "DL2", "aL1", "bL1", "cL0", "DL3", "aL2", "bL2", "cL1",
+     "aL3", "aL4", "dL0", "bL3", "cL2", "bL4", "dL1", "eL0", "cL3", "eL1", "dL2", "cL4", "dL3", "eL2", "dL4",
+     "eL3", "nL0", "nL1", "nL2", "nL4", "fL0", "fL1", "fL2", "fL3"),
 )
 
 
@@ -412,8 +504,8 @@
     nz = SUB // 2
     cols = width // nz
     fine = feat // PIECES
-    wide = 2 * fine
-    n, pieces = len(UNITS), 2 * PIECES
+    wide = 4 * fine
+    n, pieces = len(UNITS["L"]), PIECES
     dma = pltpu.SemaphoreType.DMA
     vmem = pl.BlockSpec(memory_space=pltpu.VMEM)
     hbm = pl.BlockSpec(memory_space=pltpu.HBM)
@@ -430,11 +522,14 @@
         yb=((pieces, nz, rows, wide), BF16), yr=((pieces, nz, rows, wide), BF16),
         fb=((pieces, nz, 2, rows, wide), BF16), fr=((pieces, nz, 2, rows, wide), BF16),
         kept=((PIECES, nz, rows, wide), F32), zb=((PIECES, nz, rows, wide), BF16),
-        zc=((PIECES, rows, wide), BF16), zr=((PIECES, 3, rows, wide), BF16),
+        zc=((PIECES, 2, rows, wide // 2), BF16), zr=((PIECES, 2, rows, wide), BF16),
+        zx=((PIECES, rows, wide // 2), BF16), own=((PIECES, rows, wide // 2), F32),
+        ho=((PIECES, rows, wide // 2), F32), hi=((PIECES, rows, wide // 2), F32),
     )
     sems = dict(
-        s_in=(3,), s_out=(4,), r_tz=(nz,), r_tx=(nz,), r_ty=(nz, 2), r_tc=(1,), r_ux=(nz,), r_up=(2,),
+        s_in=(3,), s_out=(6,), r_tz=(nz,), r_tx=(nz,), r_ty=(nz, 2), r_tc=(1,), r_ux=(nz,), r_up=(2,),
         r_dx=(PIECES + 1,), r_de=(1,), r_dl=(PIECES,), r_c=(n,), r_x=(n,), r_y=(n,), r_z=(PIECES, 2),
+        r_zx=(PIECES,), r_h=(PIECES,),
     )
     names = list(arrays) + list(sems)
     up_s, dn_s, mixed = pl.pallas_call(

time: 80.5 us -> 77.4 us (0.961)
  Pallas kernels: 79.7 us -> 76.6 us
    pallas_call x1, Pallas kernels: 78.3 us -> 75.2 us  [on_device_fused(): pl.pallas_call(functools.partial(fused, nz, names), out_shape=(pltpu.VMEM...]
where the time goes in v3:
time: 77.4 us; the launch traced here: 77.2 us
  Pallas kernels  76.6 us (99%)
    pallas_call x1, Pallas kernels, on_device_fused(): pl.pallas_call(functools.partial(fused, nz, names), out_shape=(pltpu.VMEM...  75.2 us

profile of v3, /device:TPU:0, one launch (start us, length us, event | category | flops | bytes accessed | tf_op | source)
XLA Modules:
  0.0 77.2 jit_solution(7290133152904166443)
XLA Ops:
  0.6 75.2 %shard_map.67 = (bf16[2048,256]{1,0:T(8,128)(2,1)S(1)}, bf16[2048,256]{1,0:T(8,128)(2,1)S(1)}, bf16[128,512]{1,0:T(8,128)(2,1)S(1)}) custom-call(bf16[128,2048]{1,0:T(8,128)(2,1)} %tok_h.1, f32[1,256]{1,0:T(1,128)} %bitcast.3, f32[256,2048]{1,0:T(8,128)} %upm_h.1, f32[256,2048]{1,0:T(8,128)} %dnm_h.1), custom_call_target="tpu_custom_call" | custom-call | tf_op jit(solution)/shard_map/pallas_call | solution.py:535
  75.8 1.4 %shard_map.68 = (bf16[2048,256]{1,0:T(8,128)(2,1)}, bf16[2048,256]{1,0:T(8,128)(2,1)}, bf16[128,512]{1,0:T(8,128)(2,1)}) custom-call(bf16[2048,256]{1,0:T(8,128)(2,1)S(1)} %get-tuple-element.9.refs_0_, bf16[2048,256]{1,0:T(8,128)(2,1)S(1)} %get-tuple-element.10.refs_1_, bf16[128,512]{1,0:T(8,128)(2,1)S(1)} %get-tuple-element.11.refs_2_), custom_call_target="tpu_custom_call" | custom-call | tf_op jit(solution)/shard_map/pallas_call | solution.py:549

commit v4 on v3

--- a/solution.py
+++ b/solution.py
@@ -285,8 +285,6 @@
         @pl.loop(0, nz)
         def _(zz):
             r.pre[at_span(zz), :] = up_dot(close * 2, zz) + up_dot(close * 2 + 1, zz)
-    with mark("dnrel0"):
-        dn_relay(0)
     with mark("upfar"):
         arrived(blocks_of(4), r.r_up.at[1])
     with mark("mmfar"):
@@ -296,7 +294,11 @@
             total = r.pre[at_span(zz), :] + up_dot(low, zz) + up_dot(low + 1, zz)
             r.act[at_span(zz), :] = jnp.square(jnp.maximum(total, 0.0)).astype(BF16)
 
-    at_pair, at_same = at_z(pair), at_z(same)
+    with mark("dnrel0"):
+        dn_relay(0)
+
+    at_pair = at_z(pair)
+    opposite, passed_on = 3 - z, 3 - pair
     my_half = (1 - c) * close + c * (1 - close)
     ours, theirs = y == my_half, y != my_half
     first_core = c == 0
@@ -401,20 +403,30 @@
                 r.zb[j, zz] = total.astype(BF16)
 
             over(base, n, body)
-            for m, who in ((0, across), (1, pair)):
+            for m, who in ((0, passed_on), (1, pair)):
                 if part != ("near", "far")[m]:
                     send(r.zb.at[j, who], r.zr.at[j, m], OURS, r.r_z.at[j, m], at_pair)
 
-    def cross_sum(kind, u):
+    def cross_sum(kind, u, where=None):
         j = UNITS[kind][u][0]
-
-        @pl.when(ours)
+        here = ours if where is None else jnp.logical_and(ours, where)
+
+        @pl.when(here)
         def _():
             arrived(r.zr.at[j, 0], r.r_z.at[j, 0])
-            total = (r.kept[j, same] + r.zr[j, 0].astype(F32)).astype(BF16)
+            total = (r.kept[j, opposite] + r.zr[j, 0].astype(F32)).astype(BF16)
             for cc in range(2):
                 r.zc[j, cc] = total[:, cc * half_wide:(cc + 1) * half_wide]
-                send(r.zc.at[j, cc], r.zx.at[j], OURS, r.r_zx.at[j], (same * 2 + x, y * 2 + cc))
+                remote(r.zc.at[j, cc], r.zx.at[j], OURS, r.r_zx.at[j], (opposite * 2 + x, y * 2 + cc),
+                       where is not at_end).start()
+
+    at_end = jnp.logical_not(central)
+
+    def central_cross(kind, u):
+        cross_sum(kind, u, central)
+
+    def end_cross(kind, u):
+        cross_sum(kind, u, at_end)
 
     def near_sum(kind, u):
         j = UNITS[kind][u][0]
@@ -448,7 +460,8 @@
         dn_relay(p)
 
     stages = dict(
-        a=product, b=core_sum, c=first_sum, d=second_sum, e=cross_sum, n=near_sum, f=last_sum, D=more_down)
+        a=product, b=core_sum, c=first_sum, d=second_sum, e=cross_sum, i=central_cross, o=end_cross,
+        n=near_sum, f=last_sum, D=more_down)
 
     seen = set()
 
@@ -486,14 +499,14 @@
     "E": tuple((j, "all") for j in range(PIECES)),
     "L": tuple((j, "all") for j in range(PIECES - 1)) + ((PIECES - 1, "far"), (PIECES - 1, "near")),
 }
-Y_FIRST = {"E": (0,), "L": (0,)}
+Y_FIRST = {"E": (1,), "L": (0,)}
 ORDER = (
-    ("DE1", "aE0", "aE1", "bE0", "aE2", "bE1", "aE3", "bE2", "DE2", "aL0", "bE3", "aL1", "DE3", "cE1", "cE0",
-     "cE2", "aL2", "dE1", "cE3", "aL3", "aL4", "dE2", "dE0", "dE3", "eE1", "eE2", "eE0", "eE3", "nE1", "nE2",
-     "nE0", "nE3", "fE0", "fE1", "fE2", "fE3"),
+    ("DE1", "aE0", "aE1", "bE0", "aE2", "bE1", "aE3", "bE2", "DE2", "aL0", "bE3", "aL1", "DE3", "cE0", "cE1",
+     "aL2", "cE2", "dE0", "aL3", "aL4", "cE3", "dE1", "dE2", "dE3", "eE0", "eE1", "eE2", "eE3", "nE0", "nE1",
+     "nE2", "nE3", "fE0", "fE1", "fE2", "fE3"),
     ("DL1", "aE0", "aE1", "aE2", "aE3", "aL0", "bL0", "DL2", "aL1", "bL1", "cL0", "DL3", "aL2", "bL2", "cL1",
-     "aL3", "aL4", "dL0", "bL3", "cL2", "bL4", "dL1", "eL0", "cL3", "eL1", "dL2", "cL4", "dL3", "eL2", "dL4",
-     "eL3", "nL0", "nL1", "nL2", "nL4", "fL0", "fL1", "fL2", "fL3"),
+     "aL3", "bL3", "aL4", "bL4", "dL0", "dL1", "cL2", "eL0", "cL3", "eL1", "dL2", "cL4", "oL2", "dL3", "oL3",
+     "dL4", "iL2", "iL3", "nL0", "nL1", "nL2", "nL4", "fL0", "fL1", "fL2", "fL3"),
 )
 
 

time: 77.4 us -> 75.4 us (0.974)
  Pallas kernels: 76.6 us -> 74.6 us
    pallas_call x1, Pallas kernels: 75.2 us -> 73.2 us  [on_device_fused(): pl.pallas_call(functools.partial(fused, nz, names), out_shape=(pltpu.VMEM...]
where the time goes in v4:
time: 75.4 us; the launch traced here: 75.2 us
  Pallas kernels  74.6 us (99%)
    pallas_call x1, Pallas kernels, on_device_fused(): pl.pallas_call(functools.partial(fused, nz, names), out_shape=(pltpu.VMEM...  73.2 us

profile of v4, /device:TPU:0, one launch (start us, length us, event | category | flops | bytes accessed | tf_op | source)
XLA Modules:
  0.0 75.2 jit_solution(12905492714524395773)
XLA Ops:
  0.6 73.2 %shard_map.67 = (bf16[2048,256]{1,0:T(8,128)(2,1)S(1)}, bf16[2048,256]{1,0:T(8,128)(2,1)S(1)}, bf16[128,512]{1,0:T(8,128)(2,1)S(1)}) custom-call(bf16[128,2048]{1,0:T(8,128)(2,1)} %tok_h.1, f32[1,256]{1,0:T(1,128)} %bitcast.3, f32[256,2048]{1,0:T(8,128)} %upm_h.1, f32[256,2048]{1,0:T(8,128)} %dnm_h.1), custom_call_target="tpu_custom_call" | custom-call | tf_op jit(solution)/shard_map/pallas_call | solution.py:548
  73.8 1.4 %shard_map.68 = (bf16[2048,256]{1,0:T(8,128)(2,1)}, bf16[2048,256]{1,0:T(8,128)(2,1)}, bf16[128,512]{1,0:T(8,128)(2,1)}) custom-call(bf16[2048,256]{1,0:T(8,128)(2,1)S(1)} %get-tuple-element.9.refs_0_, bf16[2048,256]{1,0:T(8,128)(2,1)S(1)} %get-tuple-element.10.refs_1_, bf16[128,512]{1,0:T(8,128)(2,1)S(1)} %get-tuple-element.11.refs_2_), custom_call_target="tpu_custom_call" | custom-call | tf_op jit(solution)/shard_map/pallas_call | solution.py:562

commit v5 on v4

--- a/solution.py
+++ b/solution.py
@@ -100,12 +100,15 @@
         out[pl.ds(pl.multiple_of(f * feat, feat), feat), :] = (
             block if factor is None else factor * block).astype(BF16)
 
+    def normed(q):
+        part = r.tok[:, pl.ds(pl.multiple_of(q * cols, cols), cols)].astype(F32)
+        r.xg[slot(q, z, x)] = (part * scale).astype(BF16)
+
     with mark("norm"):
         fetch[0].wait()
         full = r.tok[...].astype(F32)
         scale = lax.rsqrt(jnp.mean(full * full, axis=1, keepdims=True) + EPS)
-        for q in range(nz):
-            r.xg[slot(q, z, x)] = (full[:, q * cols:(q + 1) * cols] * scale).astype(BF16)
+        normed(t)
     with mark("barrier"):
         pl.semaphore_wait(barrier, 5)
 
@@ -176,6 +179,8 @@
     for to in (inner, pair):
         hop(t, z, x, r.r_tz.at[z], at_z(to)).start()
     over_x["own"].start()
+    for step in range(1, nz):
+        normed((t + step) % nz)
     with mark("castup"):
         fetch[1].wait()
         cast(r.upm, r.up_s, r.up_o, jnp.transpose(gain[...]))
@@ -504,7 +509,7 @@
     ("DE1", "aE0", "aE1", "bE0", "aE2", "bE1", "aE3", "bE2", "DE2", "aL0", "bE3", "aL1", "DE3", "cE0", "cE1",
      "aL2", "cE2", "dE0", "aL3", "aL4", "cE3", "dE1", "dE2", "dE3", "eE0", "eE1", "eE2", "eE3", "nE0", "nE1",
      "nE2", "nE3", "fE0", "fE1", "fE2", "fE3"),
-    ("DL1", "aE0", "aE1", "aE2", "aE3", "aL0", "bL0", "DL2", "aL1", "bL1", "cL0", "DL3", "aL2", "bL2", "cL1",
+    ("DL1", "aE0", "aE1", "aE2", "aL0", "aE3", "bL0", "DL2", "aL1", "bL1", "cL0", "DL3", "aL2", "bL2", "cL1",
      "aL3", "bL3", "aL4", "bL4", "dL0", "dL1", "cL2", "eL0", "cL3", "eL1", "dL2", "cL4", "oL2", "dL3", "oL3",
      "dL4", "iL2", "iL3", "nL0", "nL1", "nL2", "nL4", "fL0", "fL1", "fL2", "fL3"),
 )

time: 75.4 us -> 75.4 us (level)
  no operation moved by 1% of the time
where the time goes in v5:
time: 75.4 us; the launch traced here: 75.2 us
  Pallas kernels  74.6 us (99%)
    pallas_call x1, Pallas kernels, on_device_fused(): pl.pallas_call(functools.partial(fused, nz, names), out_shape=(pltpu.VMEM...  73.2 us

profile of v5, /device:TPU:0, one launch (start us, length us, event | category | flops | bytes accessed | tf_op | source)
XLA Modules:
  0.0 75.2 jit_solution(14857572634802019221)
XLA Ops:
  0.6 73.2 %shard_map.67 = (bf16[2048,256]{1,0:T(8,128)(2,1)S(1)}, bf16[2048,256]{1,0:T(8,128)(2,1)S(1)}, bf16[128,512]{1,0:T(8,128)(2,1)S(1)}) custom-call(bf16[128,2048]{1,0:T(8,128)(2,1)} %tok_h.1, f32[1,256]{1,0:T(1,128)} %bitcast.3, f32[256,2048]{1,0:T(8,128)} %upm_h.1, f32[256,2048]{1,0:T(8,128)} %dnm_h.1), custom_call_target="tpu_custom_call" | custom-call | tf_op jit(solution)/shard_map/pallas_call | solution.py:553
  73.8 1.4 %shard_map.68 = (bf16[2048,256]{1,0:T(8,128)(2,1)}, bf16[2048,256]{1,0:T(8,128)(2,1)}, bf16[128,512]{1,0:T(8,128)(2,1)}) custom-call(bf16[2048,256]{1,0:T(8,128)(2,1)S(1)} %get-tuple-element.9.refs_0_, bf16[2048,256]{1,0:T(8,128)(2,1)S(1)} %get-tuple-element.10.refs_1_, bf16[128,512]{1,0:T(8,128)(2,1)S(1)} %get-tuple-element.11.refs_2_), custom_call_target="tpu_custom_call" | custom-call | tf_op jit(solution)/shard_map/pallas_call | solution.py:567
